TPU v7x, 32 devices: a whole 2x2x4 slice. The times are simulated.
32 devices in a mesh: sp: 16 (over z, y, x), tp: 2 (over core).
Axes of the slice: x: 2, y: 2, z: 4, core: 2. Of those that a mesh axis runs over, the one named last changes fastest.
Arguments:
- latent: bfloat16 [4096, 2048], P(('sp', 'tp')), may hold values from -6 to 6
- context: bfloat16 [512, 2048], P('sp'), may hold values from -6 to 6
- condition: float32 [2048], P('tp'), may hold values from -6 to 6
- context_condition: float32 [2048], P('tp'), may hold values from -6 to 6
- modulation_weight: bfloat16 [2048, 6144], P('tp', 'sp'), may hold values from -0.125 to 0.125
- query_first: bfloat16 [2048, 512], P(None, 'tp'), may hold values from -1 to 1
- query_second: bfloat16 [2048, 512], P(None, 'tp'), may hold values from -1 to 1
- key_first: bfloat16 [2048, 512], P(None, 'tp'), may hold values from -1 to 1
- key_second: bfloat16 [2048, 512], P(None, 'tp'), may hold values from -1 to 1
- value_weight: bfloat16 [2048, 1024], P(None, 'tp'), may hold values from -0.125 to 0.125
- lambda_head: float32 [8], P('tp'), may hold values from 0.3 to 0.8
- context_score_boost: float32 [8], P('tp'), may hold values from 1.5 to 3
- head_gain: float32 [128], replicated, may hold values from 0.1 to 1.9
- output_weight: bfloat16 [1024, 2048], P('tp'), may hold values from -0.1875 to 0.1875
Outputs:
- updated: bfloat16 [4096, 2048], P(('sp', 'tp'))
All inputs are finite; a program needn't handle non-finite values.
Results may differ from a plain program's by a relative error of at most 0.0095.
Values may be sent and summed in bfloat16 or wider, within the bound.
A program may use at most 64 MiB of HBM per device.

v0:
```python
import functools
import math

import jax
import jax.numpy as jnp
import numpy as np
from jax import lax
from jax.experimental import pallas as pl
from jax.experimental.pallas import tpu as pltpu
from jax.sharding import PartitionSpec as P

HEAD_DIM = 64
VALUE_DIM = 128
GRID_W = 64
EPSILON = 1e-06
THETA = 10000.0
NEGATIVE = -1e30
LOG2E = math.log2(math.e)
MESH = pl.DeviceIdType.MESH
BF16 = jnp.bfloat16
F32 = jnp.float32
LANES = 128
QROWS = 256


def rotation_tables(grid_rows):
    half = HEAD_DIM // 2
    quarter = half // 2
    lane = np.arange(LANES) % HEAD_DIM
    rate = (THETA ** (-(lane % quarter) / quarter)).astype(np.float32)
    sign = np.where(lane % half < quarter, -1.0, 1.0)
    tables = []
    for count, mask in ((grid_rows, lane < half), (GRID_W, lane >= half)):
        angle = np.arange(count, dtype=np.float32)[:, None] * rate[None, :]
        for table in (np.cos(angle), np.sin(angle) * sign):
            tables.append(np.where(mask, table, 0.0).astype(np.float32))
    return tables


def rotate(x, cosine, sine):
    quarter = HEAD_DIM // 4
    lane = lax.broadcasted_iota(jnp.int32, x.shape, 1)
    ahead = pltpu.roll(x, LANES - quarter, 1)
    behind = pltpu.roll(x, quarter, 1)
    flipped = jnp.where(lane % (2 * quarter) < quarter, ahead, behind)
    return x * cosine + flipped * sine


def normed_rows(rows):
    v = rows.astype(F32)
    return v * lax.rsqrt(jnp.mean(v * v, axis=-1, keepdims=True) + EPSILON)


def kernel(
    dims,
    latent_ref, context_ref, cond_ref, ccond_ref, modw_ref,
    wq1_hbm, wq2_hbm, wk1_hbm, wk2_hbm, wv_hbm,
    lam_ref, boost_ref, gain_ref, wo_hbm, crow_ref, srow_ref, ccol_ref, scol_ref,
    out_ref,
    wq1, wq2, wk1, wk2, wv, wo,
    cos_ref, sin_ref, sig, modp, modall, modrow, lat, nrm, h,
    qs, kvs, q, kv, mx, acc, ho, hr, rsend, rs,
    wsem, mp_s, mp_r, lt_s, lt_r, ma_s, ma_r,
    q_s, q_r, kz_s, kv_s, kv_r, ho_s, ho_r, rs_s, rs_r,
):
    S, T, G, R, B, Cr, cw = dims
    s, t = lax.axis_index("sp"), lax.axis_index("tp")
    g, r = s // R, s % R
    rows, D = latent_ref.shape
    Lr = rows * T
    Cp = context_ref.shape[0]

    def remote(src, dst, send, recv, sp, tp):
        return pltpu.make_async_remote_copy(
            src_ref=src, dst_ref=dst, send_sem=send, recv_sem=recv,
            device_id=(sp, tp), device_id_type=MESH,
        )

    loads = [
        pltpu.make_async_copy(a, b, wsem.at[i])
        for i, (a, b) in enumerate(
            [(wq1_hbm, wq1), (wq2_hbm, wq2), (wk1_hbm, wk1), (wk2_hbm, wk2), (wv_hbm, wv), (wo_hbm, wo)]
        )
    ]
    for load in loads:
        load.start()

    barrier = pltpu.get_barrier_semaphore()

    @pl.loop(1, S)
    def _(i):
        pl.semaphore_signal(barrier, inc=1, device_id=((s + i) % S, t), device_id_type=MESH)

    for i in range(1, T):
        pl.semaphore_signal(barrier, inc=1, device_id=(s, (t + i) % T), device_id_type=MESH)

    for i in range(Lr // GRID_W):
        span, at = slice(i * GRID_W, (i + 1) * GRID_W), pl.ds(s * (Lr // GRID_W) + i, 1)
        cos_ref[span, :] = ccol_ref[...] + crow_ref[at, :]
        sin_ref[span, :] = scol_ref[...] + srow_ref[at, :]
    cos_ref[Lr:, :] = jnp.ones((Cp, LANES), F32)
    sin_ref[Lr:, :] = jnp.zeros((Cp, LANES), F32)

    for i, ref in enumerate((cond_ref, ccond_ref)):
        v = ref[...]
        sig[i : i + 1, :] = v / (1.0 + jnp.exp(-v))
    modp[t] = jnp.dot(sig[...].astype(BF16), modw_ref[...], preferred_element_type=F32)

    pl.semaphore_wait(barrier, S - 1 + T - 1)

    def part_copy(i):
        return remote(modp.at[t], modp.at[t], mp_s.at[i], mp_r.at[t], s, (t + i) % T)

    def latent_copy(i):
        return remote(latent_ref, lat.at[t], lt_s.at[i], lt_r.at[t], s, (t + i) % T)

    for i in range(1, T):
        part_copy(i).start()
    for i in range(1, T):
        latent_copy(i).start()
    lat[t] = latent_ref[...]
    for i in range(1, T):
        o = (t + i) % T
        remote(modp.at[o], modp.at[o], mp_s.at[i], mp_r.at[o], s, o).wait_recv()
    total = modp[0]
    for i in range(1, T):
        total = total + modp[i]
    modall[s] = total

    def mod_copy(i, src):
        return remote(modall.at[src], modall.at[src], ma_s.at[i], ma_r.at[src], (s + i) % S, t)

    @pl.loop(1, S)
    def _(i):
        mod_copy(i, s).start()

    for i in range(1, T):
        o = (t + i) % T
        remote(lat.at[o], lat.at[o], lt_s.at[i], lt_r.at[o], s, o).wait_recv()
    step = math.gcd(rows, 32)
    for i in range(T):

        @pl.loop(0, rows // step)
        def _(j):
            at = pl.multiple_of(j * step, step)
            nrm[pl.ds(i * rows + at, step), :] = normed_rows(lat[i, pl.ds(at, step), :])

    nrm[Lr:, :] = normed_rows(context_ref[...])

    @pl.loop(1, S)
    def _(i):
        mod_copy(i, (s + i) % S).wait_recv()

    for i in range(S):
        modrow[:, i * cw : (i + 1) * cw] = modall[i][:, :cw]

    @pl.loop(0, Lr // step)
    def _(j):
        at = pl.ds(pl.multiple_of(j * step, step), step)
        h[at, :] = (nrm[at, :] * (1.0 + modrow[0:1, D : 2 * D]) + modrow[0:1, :D]).astype(BF16)

    h[Lr:, :] = (nrm[Lr:, :] * (1.0 + modrow[1:2, D : 2 * D]) + modrow[1:2, :D]).astype(BF16)

    for i in range(2):
        loads[i].wait()
    lh = h[:Lr, :]
    one = jnp.dot(lh, wq1[...], preferred_element_type=F32)
    two = jnp.dot(lh, wq2[...], preferred_element_type=F32)
    for i in range(G):
        cut = slice(i * HEAD_DIM, (i + 1) * HEAD_DIM)
        pair = jnp.concatenate([one[:, cut], two[:, cut]], axis=1)
        turned = rotate(pair, cos_ref[:Lr, :], sin_ref[:Lr, :])
        qs[i] = (turned * (LOG2E * HEAD_DIM**-0.5)).astype(BF16)

    def q_out(i):
        to = (g + i) % G
        return remote(qs.at[to], q.at[g], q_s.at[i], q_r.at[g], to * R + r, t)

    for i in range(1, G):
        q_out(i).start()
    q[g] = qs[g]

    for i in range(2, 5):
        loads[i].wait()
    hh = h[...]
    one = jnp.dot(hh, wk1[...], preferred_element_type=F32)
    two = jnp.dot(hh, wk2[...], preferred_element_type=F32)
    for i in range(G):
        cut = slice(i * HEAD_DIM, (i + 1) * HEAD_DIM)
        pair = jnp.concatenate([one[:, cut], two[:, cut]], axis=1)
        kvs[i, :, :LANES] = rotate(pair, cos_ref[...], sin_ref[...]).astype(BF16)
    val = jnp.dot(hh, wv[...], preferred_element_type=F32)
    for i in range(G):
        kvs[i, :, LANES:] = val[:, i * VALUE_DIM : (i + 1) * VALUE_DIM].astype(BF16)

    def kv_out(i):
        to = (g + i) % G
        return remote(kvs.at[to], kv.at[s], kz_s.at[i], kv_r.at[s], to * R + r, t)

    for i in range(1, G):
        kv_out(i).start()
    kv[s] = kvs[g]

    def forward(i, j):
        src = ((g + G - i) % G) * R + r
        return remote(kv.at[src], kv.at[src], kv_s.at[i, j], kv_r.at[src], g * R + (r + j) % R, t)

    def landed(src):
        remote(kv.at[src], kv.at[src], kz_s.at[0], kv_r.at[src], s, t).wait_recv()

    def forward_all(i):
        @pl.loop(1, R)
        def _(j):
            forward(i, j).start()

    forward_all(0)
    mx[...] = jnp.full(mx.shape, NEGATIVE, F32)
    acc[...] = jnp.zeros(acc.shape, F32)
    boost = boost_ref[g] * LOG2E

    for i in range(1, G):
        o = (g + i) % G
        remote(q.at[o], q.at[o], q_s.at[i], q_r.at[o], s, t).wait_recv()

    def attend(n, at):
        k_l = kv[pl.ds(at, B), :Lr, :LANES].reshape(B * Lr, LANES)
        v_l = kv[pl.ds(at, B), :Lr, LANES:].reshape(B * Lr, VALUE_DIM)
        k_c = kv[pl.ds(at, B), Lr:, :LANES].reshape(B * Cp, LANES)
        v_c = kv[pl.ds(at, B), Lr:, LANES:].reshape(B * Cp, VALUE_DIM)
        v_l = jnp.concatenate([v_l, jnp.ones_like(v_l)], axis=1)
        v_c = jnp.concatenate([v_c, jnp.ones_like(v_c)], axis=1)
        nt = (((1,), (1,)), ((), ()))
        QB = min(Lr, QROWS)
        for m, c in [(m, c) for c in range(Lr // QB) for m in range(2)]:
            part = slice(c * QB, (c + 1) * QB)
            qq = q[n, part, :]
            lane = lax.broadcasted_iota(jnp.int32, qq.shape, 1)
            qm = jnp.where(lane // HEAD_DIM == m, qq, jnp.zeros_like(qq))
            s_l = lax.dot_general(qm, k_l, nt, preferred_element_type=F32)
            s_c = lax.dot_general(qm, k_c, nt, preferred_element_type=F32) + boost
            if Cp != Cr:
                spot = lax.broadcasted_iota(jnp.int32, s_c.shape, 1)
                s_c = jnp.where(spot % Cp < Cr, s_c, NEGATIVE)
            old = mx[m, n, part, :]
            peak = jnp.maximum(
                old,
                jnp.maximum(
                    jnp.max(s_l, axis=-1, keepdims=True), jnp.max(s_c, axis=-1, keepdims=True)
                ),
            )
            p_l = jnp.exp2(s_l - peak).astype(BF16)
            p_c = jnp.exp2(s_c - peak).astype(BF16)
            mx[m, n, part, :] = peak
            acc[m, n, part, :] = (
                jnp.exp2(old - peak) * acc[m, n, part, :]
                + jnp.dot(p_l, v_l, preferred_element_type=F32)
                + jnp.dot(p_c, v_c, preferred_element_type=F32)
            )

    lam = lam_ref[g]
    gain = gain_ref[...]

    def finish(n):
        one = acc[0, n, :, :VALUE_DIM] / acc[0, n, :, VALUE_DIM:]
        two = acc[1, n, :, :VALUE_DIM] / acc[1, n, :, VALUE_DIM:]
        mixed = one - lam * two
        mixed = mixed * lax.rsqrt(jnp.mean(mixed * mixed, axis=-1, keepdims=True) + EPSILON) * gain
        return mixed.astype(BF16)

    def ho_out(i):
        to = (g + i) % G
        return remote(ho.at[to], hr.at[g], ho_s.at[i], ho_r.at[g], to * R + r, t)

    def pass_on(i):
        landed(((g + G - i) % G) * R + r)
        forward_all(i)

    for i in range(G):
        if i == 1 and G > 2:
            pass_on(2)
        base = ((g + G - i) % G) * R

        @pl.loop(1, R)
        def _(j):
            landed(base + (r + j) % R)

        if i + 1 < G:
            half = G // 2
            for low, high in ((0, half), (half, G)):
                if low and i == 0:
                    pass_on(1)
                elif low and i + 2 < G:
                    pass_on(i + 2)

                @pl.loop(low * (R // B), high * (R // B))
                def _(x):
                    attend(x // (R // B), base + x % (R // B) * B)

        else:

            @pl.loop(1, G + 1)
            def _(y):
                n = (g + y) % G

                @pl.loop(0, R // B)
                def _(x):
                    attend(n, base + x * B)

                ho[n] = finish(n)

                @pl.when(y < G)
                def _():
                    ho_out(y).start()

    hr[g] = ho[g]
    loads[5].wait()
    for i in range(1, G):
        o = (g + i) % G
        remote(hr.at[o], hr.at[o], ho_s.at[i], ho_r.at[o], s, t).wait_recv()

    def branch_rows(o):
        at = pl.multiple_of(o * rows, rows)
        mine = jnp.concatenate([hr[i, pl.ds(at, rows), :] for i in range(G)], axis=1)
        return jnp.dot(mine, wo[...], preferred_element_type=F32)

    def rs_out(i):
        o = (t + i) % T
        return remote(rsend.at[o], rs.at[t], rs_s.at[i], rs_r.at[t], s, o)

    for i in range(1, T):
        o = (t + i) % T
        rsend[o] = branch_rows(o).astype(BF16)
        rs_out(i).start()
    branch = branch_rows(t)
    for i in range(1, T):
        o = (t + i) % T
        remote(rs.at[o], rs.at[o], rs_s.at[i], rs_r.at[o], s, o).wait_recv()
        branch = branch + rs[o].astype(F32)
    out_ref[...] = (latent_ref[...].astype(F32) + modrow[0:1, 2 * D :] * branch).astype(BF16)

    for i in range(1, T):
        part_copy(i).wait_send()
        latent_copy(i).wait_send()
        rs_out(i).wait_send()

    @pl.loop(1, S)
    def _(i):
        mod_copy(i, s).wait_send()

    for i in range(1, G):
        kv_out(i).wait_send()
        q_out(i).wait_send()
        ho_out(i).wait_send()
    for i in range(G):

        @pl.loop(1, R)
        def _(j):
            forward(i, j).wait_send()


def body(
    S, T,
    latent, context, condition, context_condition, modulation_weight,
    query_first, query_second, key_first, key_second, value_weight,
    lambda_head, context_score_boost, head_gain, output_weight,
):
    rows, D = latent.shape
    Lr = rows * T
    G = value_weight.shape[1] // VALUE_DIM
    assert S % G == 0
    R = S // G
    B = math.gcd(R, 4)
    Cr = context.shape[0]
    Cp = -(-Cr // 16) * 16
    if Cp != Cr:
        context = jnp.pad(context, ((0, Cp - Cr), (0, 0)))
    cw = modulation_weight.shape[1]
    cp = -(-cw // LANES) * LANES
    if cp != cw:
        modulation_weight = jnp.pad(modulation_weight, ((0, 0), (0, cp - cw)))
    depth = modulation_weight.shape[0]
    assert Lr % GRID_W == 0
    tables = rotation_tables(S * Lr // GRID_W)
    vm = pl.BlockSpec(memory_space=pltpu.VMEM)
    sm = pl.BlockSpec(memory_space=pltpu.SMEM)
    hb = pl.BlockSpec(memory_space=pl.ANY)
    V = pltpu.VMEM
    dma = pltpu.SemaphoreType.DMA
    weights = (query_first, query_second, key_first, key_second, value_weight, output_weight)
    return pl.pallas_call(
        functools.partial(kernel, (S, T, G, R, B, Cr, cw)),
        out_shape=jax.ShapeDtypeStruct((rows, D), BF16),
        in_specs=[vm] * 5 + [hb] * 5 + [sm, sm, vm, hb, vm, vm, vm, vm],
        out_specs=vm,
        scratch_shapes=[V(w.shape, BF16) for w in weights]
        + [
            V((Lr + Cp, LANES), F32),
            V((Lr + Cp, LANES), F32),
            V((2, depth), F32),
            V((T, 2, cp), F32),
            V((S, 2, cp), F32),
            V((2, 3 * D), F32),
            V((T, rows, D), BF16),
            V((Lr + Cp, D), F32),
            V((Lr + Cp, D), BF16),
            V((G, Lr, LANES), BF16),
            V((G, Lr + Cp, LANES + VALUE_DIM), BF16),
            V((G, Lr, LANES), BF16),
            V((S, Lr + Cp, LANES + VALUE_DIM), BF16),
            V((2, G, Lr, 1), F32),
            V((2, G, Lr, 2 * VALUE_DIM), F32),
            V((G, Lr, VALUE_DIM), BF16),
            V((G, Lr, VALUE_DIM), BF16),
            V((T, rows, D), BF16),
            V((T, rows, D), BF16),
            dma((6,)),
            dma((T,)), dma((T,)), dma((T,)), dma((T,)), dma((S,)), dma((S,)),
            dma((G,)), dma((G,)), dma((G,)), dma((G, R)), dma((S,)),
            dma((G,)), dma((G,)), dma((T,)), dma((T,)),
        ],
        compiler_params=pltpu.CompilerParams(
            collective_id=0, has_side_effects=True, vmem_limit_bytes=62 * 1024 * 1024
        ),
    )(
        latent, context, condition[None, :], context_condition[None, :], modulation_weight,
        query_first, query_second, key_first, key_second, value_weight,
        lambda_head, context_score_boost, head_gain[None, :], output_weight, *tables,
    )


def solution(mesh):
    in_specs = (
        P(("sp", "tp"), None),
        P("sp", None),
        P("tp"),
        P("tp"),
        P("tp", "sp"),
        P(None, "tp"),
        P(None, "tp"),
        P(None, "tp"),
        P(None, "tp"),
        P(None, "tp"),
        P("tp"),
        P("tp"),
        P(),
        P("tp", None),
    )
    out_specs = P(("sp", "tp"), None)
    run = functools.partial(body, mesh.shape["sp"], mesh.shape["tp"])
    return jax.shard_map(run, mesh=mesh, in_specs=in_specs, out_specs=out_specs, check_vma=False)
```

profile of v0, /device:TPU:1, one launch (start us, length us, event | category | flops | bytes accessed | tf_op | source)
XLA Modules:
  0.0 64.6 jit_solution(16930760007500322690)
XLA Ops:
  0.0 62.7 %shard_map.172 = bf16[128,2048]{1,0:T(8,128)(2,1)} custom-call(bf16[128,2048]{1,0:T(8,128)(2,1)} %latent_ref.1, bf16[32,2048]{1,0:T(8,128)(2,1)} %context_ref.1, f32[1,1024]{1,0:T(1,128)} %bitcast.3, f32[1,1024]{1,0:T(1,128)} %bitcast.4, bf16[1024,384]{1,0:T(8,128)(2,1)} %modw_ref.1, bf16[2048,256]{1,0:T(8,128)(2,1)} %wq1_hbm.1, bf16[2048,256]{1,0:T(8,128)(2,1)} %wq2_hbm.1, ...), custom_call_target="tpu_custom_call" | custom-call | tf_op jit(solution)/shard_map/pallas_call | solution.py:390
  62.7 1.9 %copy.20 = bf16[128,2048]{1,0:T(8,128)(2,1)} copy(bf16[128,2048]{1,0:T(8,128)(2,1)} %shard_map.172) | data formatting | bytes 1048576
where the time goes:
time: 64.8 us; the launch traced here: 64.6 us
  Pallas kernels  62.7 us (97%)
  local copies, waits for them, and re-layouts  1.88 us (3%)
    pallas_call x1, Pallas kernels, body(): pl.pallas_call(functools.partial(kernel, (S, T, G, R, B, Cr, cw)), out_sh...  62.7 us
    unnamed x1, local copies, waits for them, and re-layouts  1.88 us

commit v1 on v0

v1 whole, which is shorter than its diff:
```python
import functools
import math

import jax
import jax.numpy as jnp
import numpy as np
from jax import lax
from jax.experimental import pallas as pl
from jax.experimental.pallas import tpu as pltpu
from jax.sharding import PartitionSpec as P

HEAD_DIM = 64
VALUE_DIM = 128
GRID_W = 64
EPSILON = 1e-06
THETA = 10000.0
NEGATIVE = -1e30
LOG2E = math.log2(math.e)
MESH = pl.DeviceIdType.MESH
BF16 = jnp.bfloat16
F32 = jnp.float32
LANES = 128


def rotation_tables(grid_rows):
    half = HEAD_DIM // 2
    quarter = half // 2
    lane = np.arange(LANES) % HEAD_DIM
    rate = (THETA ** (-(lane % quarter) / quarter)).astype(np.float32)
    sign = np.where(lane % half < quarter, -1.0, 1.0)
    tables = []
    for count, mask in ((grid_rows, lane < half), (GRID_W, lane >= half)):
        angle = np.arange(count, dtype=np.float32)[:, None] * rate[None, :]
        for table in (np.cos(angle), np.sin(angle) * sign):
            tables.append(np.where(mask, table, 0.0).astype(np.float32))
    return tables


def rotate(x, cosine, sine):
    quarter = HEAD_DIM // 4
    lane = lax.broadcasted_iota(jnp.int32, x.shape, 1)
    ahead = pltpu.roll(x, LANES - quarter, 1)
    behind = pltpu.roll(x, quarter, 1)
    flipped = jnp.where(lane % (2 * quarter) < quarter, ahead, behind)
    return x * cosine + flipped * sine


def normed_rows(rows):
    v = rows.astype(F32)
    return v * lax.rsqrt(jnp.mean(v * v, axis=-1, keepdims=True) + EPSILON)


def flip(v, k, span):
    out = 0
    bit = 1
    while bit < span:
        out = out + bit * ((v // bit + k // bit) % 2)
        bit *= 2
    return out


def kernel(
    dims,
    lat_hbm, ctx_hbm, cond_hbm, ccond_hbm, modw_hbm,
    wq1_hbm, wq2_hbm, wk1_hbm, wk2_hbm, wv_hbm,
    lam_ref, boost_ref, gain_ref, wo_hbm, crow_ref, srow_ref, ccol_ref, scol_ref,
    out_ref,
    wq1, wq2, wk1, wk2, wv, wo,
    ctx, cond, modw, cos_ref, sin_ref, mp, modall, modrow, lat, nrm, h,
    qs, kvs, q, kv, vts, mx, acc, ho, hr, lb,
    wsem, isem, mp_s, mp_r, ma_s, ma_r, lt_s, lt_r, lb_s, lb_r, wo_s, wo_r,
    q_s, q_r, kz_s, kv_r, fx_s, fd_s, ho_s, ho_r,
):
    S, T, G, R, A, B, Cr, cw = dims
    P = T * G
    near = max(P // 2, 1)
    s, t = lax.axis_index("sp"), lax.axis_index("tp")
    p0, r = s // R, s % R
    a0, b0 = s // B, s % B
    prim, hown = p0 // G, p0 % G
    _, rows, D = lat.shape
    Lr = rows * T
    Cp = ctx.shape[0]

    def remote(src, dst, send, recv, sp, tp):
        return pltpu.make_async_remote_copy(
            src_ref=src, dst_ref=dst, send_sem=send, recv_sem=recv,
            device_id=(sp, tp), device_id_type=MESH,
        )

    f0 = b0 * T + t
    FB = B * T

    def plane(j):
        f = (f0 + j) % FB
        return f, a0 * B + f // T, f % T

    barrier = pltpu.get_barrier_semaphore()
    for j in range(1, FB):
        _, sp, tp = plane(j)
        pl.semaphore_signal(barrier, inc=1, device_id=(sp, tp), device_id_type=MESH)
    for i in range(1, A):
        pl.semaphore_signal(
            barrier, inc=1, device_id=((a0 + i) % A * B + b0, t), device_id_type=MESH
        )

    inputs = [
        pltpu.make_async_copy(a, b, isem.at[i])
        for i, (a, b) in enumerate(
            [(cond_hbm, cond.at[0:1]), (ccond_hbm, cond.at[1:2]), (modw_hbm, modw),
             (lat_hbm, lat.at[t]), (ctx_hbm, ctx)]
        )
    ]
    for load in inputs:
        load.start()
    loads = [
        pltpu.make_async_copy(a, b, wsem.at[i])
        for i, (a, b) in enumerate(
            [(wk1_hbm, wk1), (wk2_hbm, wk2), (wv_hbm, wv), (wq1_hbm, wq1), (wq2_hbm, wq2), (wo_hbm, wo.at[t])]
        )
    ]
    for load in loads:
        load.start()

    for i in range(G):
        lb[t, i : i + 1, :] = jnp.full((1, LANES), lam_ref[i], F32)
        lb[t, G + i : G + i + 1, :] = jnp.full((1, LANES), boost_ref[i] * LOG2E, F32)

    for i in range(3):
        inputs[i].wait()
    v = cond[...]
    sig = v / (1.0 + jnp.exp(-v))
    mp[f0] = jnp.dot(sig.astype(BF16), modw[...], preferred_element_type=F32)
    for i in range(3, 5):
        inputs[i].wait()

    pl.semaphore_wait(barrier, FB - 1 + A - 1)

    def mp_copy(j):
        _, sp, tp = plane(j)
        return remote(mp.at[f0], mp.at[f0], mp_s.at[j], mp_r.at[f0], sp, tp)

    def lat_copy(i):
        return remote(lat.at[t], lat.at[t], lt_s.at[i], lt_r.at[t], s, (t + i) % T)

    def lb_copy(i):
        return remote(lb.at[t], lb.at[t], lb_s.at[i], lb_r.at[t], s, (t + i) % T)

    def wo_copy(i):
        return remote(wo.at[t], wo.at[t], wo_s.at[i], wo_r.at[t], s, (t + i) % T)

    def from_core(buf, recv, i):
        o = (t + i) % T
        remote(buf.at[o], buf.at[o], lt_s.at[i], recv.at[o], s, o).wait_recv()

    for j in range(1, FB):
        mp_copy(j).start()
    for i in range(1, T):
        lat_copy(i).start()
        lb_copy(i).start()

    for i in range(Lr // GRID_W):
        span, at = slice(i * GRID_W, (i + 1) * GRID_W), pl.ds(s * (Lr // GRID_W) + i, 1)
        cos_ref[span, :] = ccol_ref[...] + crow_ref[at, :]
        sin_ref[span, :] = scol_ref[...] + srow_ref[at, :]
    cos_ref[Lr:, :] = jnp.ones((Cp, LANES), F32)
    sin_ref[Lr:, :] = jnp.zeros((Cp, LANES), F32)

    for j in range(1, FB):
        f, sp, tp = plane(j)
        remote(mp.at[f], mp.at[f], mp_s.at[j], mp_r.at[f], sp, tp).wait_recv()
    for b in range(B):
        total = mp[b * T]
        for i in range(1, T):
            total = total + mp[b * T + i]
        modall[a0, b] = total

    def mod_copy(i, src):
        return remote(
            modall.at[src], modall.at[src], ma_s.at[i], ma_r.at[src], (a0 + i) % A * B + b0, t
        )

    for i in range(1, A):
        mod_copy(i, a0).start()

    step = math.gcd(rows, 32)

    def norm_lat(i):
        @pl.loop(0, rows // step)
        def _(j):
            at = pl.multiple_of(j * step, step)
            nrm[pl.ds(i * rows + at, step), :] = normed_rows(lat[i, pl.ds(at, step), :])

    nrm[Lr:, :] = normed_rows(ctx[...])
    norm_lat(t)
    for i in range(1, T):
        from_core(lat, lt_r, i)
        norm_lat((t + i) % T)

    for i in range(1, A):
        mod_copy(i, (a0 + i) % A).wait_recv()
    for a in range(A):
        for b in range(B):
            i = a * B + b
            modrow[:, i * cw : (i + 1) * cw] = modall[a, b][:, :cw]

    @pl.loop(0, Lr // step)
    def _(j):
        at = pl.ds(pl.multiple_of(j * step, step), step)
        h[at, :] = (nrm[at, :] * (1.0 + modrow[0:1, D : 2 * D]) + modrow[0:1, :D]).astype(BF16)

    h[Lr:, :] = (nrm[Lr:, :] * (1.0 + modrow[1:2, D : 2 * D]) + modrow[1:2, :D]).astype(BF16)

    for i in range(3):
        loads[i].wait()
    hh = h[...]
    one = jnp.dot(hh, wk1[...], preferred_element_type=F32)
    two = jnp.dot(hh, wk2[...], preferred_element_type=F32)
    for i in range(G):
        cut = slice(i * HEAD_DIM, (i + 1) * HEAD_DIM)
        pair = jnp.concatenate([one[:, cut], two[:, cut]], axis=1)
        kvs[i, :, :LANES] = rotate(pair, cos_ref[...], sin_ref[...]).astype(BF16)
    val = jnp.dot(hh, wv[...], preferred_element_type=F32)
    for i in range(G):
        kvs[i, :, LANES:] = val[:, i * VALUE_DIM : (i + 1) * VALUE_DIM].astype(BF16)

    mine = t == prim

    def kv_out(i):
        hl = flip(hown, i, G)
        return remote(kvs.at[hl], kv.at[s], kz_s.at[i], kv_r.at[s], (t * G + hl) * R + r, t)

    @pl.when(mine)
    def _():
        kv[s] = kvs[hown]

    @pl.when(jnp.logical_not(mine))
    def _():
        kv_out(0).start()

    for i in range(1, G):
        kv_out(i).start()

    for i in range(3, 5):
        loads[i].wait()
    lh = h[:Lr, :]
    one = jnp.dot(lh, wq1[...], preferred_element_type=F32)
    two = jnp.dot(lh, wq2[...], preferred_element_type=F32)
    for i in range(G):
        cut = slice(i * HEAD_DIM, (i + 1) * HEAD_DIM)
        pair = jnp.concatenate([one[:, cut], two[:, cut]], axis=1)
        turned = rotate(pair, cos_ref[:Lr, :], sin_ref[:Lr, :])
        qs[i] = (turned * (LOG2E * HEAD_DIM**-0.5)).astype(BF16)

    def q_out(i, j):
        hl = flip(hown, i, G)
        to = (t + j) % T
        part = pl.ds(pl.multiple_of(to * rows, rows), rows)
        return remote(
            qs.at[hl, part], q.at[p0], q_s.at[i, j], q_r.at[p0], (t * G + hl) * R + r, to
        )

    @pl.when(mine)
    def _():
        q[p0] = qs[hown, pl.ds(pl.multiple_of(t * rows, rows), rows), :]

    @pl.when(jnp.logical_not(mine))
    def _():
        q_out(0, 0).start()

    for j in range(1, T):
        q_out(0, j).start()
    for i in range(1, G):
        for j in range(T):
            q_out(i, j).start()

    loads[5].wait()
    for i in range(1, T):
        wo_copy(i).start()

    def landed(src):
        remote(kv.at[src], kv.at[src], kz_s.at[0], kv_r.at[src], s, t).wait_recv()

    def to_pair(u, j):
        src = u * R + r
        return remote(kv.at[src], kv.at[src], fx_s.at[u, j], kv_r.at[src], p0 * R + (r + j) % R, t)

    def to_core(src, j):
        return remote(kv.at[src], kv.at[src], fd_s.at[src, j], kv_r.at[src], s, (t + j) % T)

    mx[...] = jnp.full(mx.shape, NEGATIVE, F32)
    acc[...] = jnp.zeros(acc.shape, F32)
    vts[:, VALUE_DIM:, :] = jnp.ones((P, vts.shape[1] - VALUE_DIM, vts.shape[2]), BF16)
    for i in range(1, T):
        from_core(lb, lb_r, i)
    lam = lb[prim, pl.ds(hown, 1), :]
    boost = lb[prim, pl.ds(G + hown, 1), :]
    boost = jnp.concatenate([boost, boost], axis=1)[:, : 2 * rows]
    gain = jnp.broadcast_to(gain_ref[...], (VALUE_DIM, LANES)).T
    nt = (((1,), (1,)), ((), ()))

    def turn_values(u):
        at = pl.ds(u * R, R)
        vals = jnp.concatenate(
            [
                kv[at, :Lr, LANES:].reshape(R * Lr, VALUE_DIM),
                kv[at, Lr:, LANES:].reshape(R * Cp, VALUE_DIM),
            ],
            axis=0,
        )
        vts[u, :VALUE_DIM, :] = vals.astype(F32).T.astype(BF16)

    def attend(blocks, u):
        at = pl.ds(u * R, R)
        keys = jnp.concatenate(
            [kv[at, :Lr, :LANES].reshape(R * Lr, LANES), kv[at, Lr:, :LANES].reshape(R * Cp, LANES)],
            axis=0,
        )
        vals = vts[u]
        for j in blocks:
            qq = q[j]
            lane = lax.broadcasted_iota(jnp.int32, qq.shape, 1)
            zero = jnp.zeros_like(qq)
            both = jnp.concatenate(
                [jnp.where(lane < HEAD_DIM, qq, zero), jnp.where(lane < HEAD_DIM, zero, qq)], axis=0
            )
            sc = lax.dot_general(keys, both, nt, preferred_element_type=F32)
            s_l, s_c = sc[: R * Lr], sc[R * Lr :] + boost
            if Cp != Cr:
                spot = lax.broadcasted_iota(jnp.int32, s_c.shape, 0)
                s_c = jnp.where(spot % Cp < Cr, s_c, NEGATIVE)
            old = mx[j]
            peak = jnp.maximum(
                old,
                jnp.maximum(
                    jnp.max(s_l, axis=0, keepdims=True), jnp.max(s_c, axis=0, keepdims=True)
                ),
            )
            pr = jnp.concatenate(
                [jnp.exp2(s_l - peak).astype(BF16), jnp.exp2(s_c - peak).astype(BF16)], axis=0
            )
            mx[j] = peak
            acc[j] = jnp.exp2(old - peak) * acc[j] + jnp.dot(vals, pr, preferred_element_type=F32)

    def finish(j):
        u = acc[j, :VALUE_DIM, :] / acc[j, VALUE_DIM : VALUE_DIM + 1, :]
        mixed = u[:, :rows] - lam[:, :rows] * u[:, rows:]
        mixed = mixed * lax.rsqrt(jnp.mean(mixed * mixed, axis=0, keepdims=True) + EPSILON)
        ho[j] = (mixed * gain[:, :rows]).T.astype(BF16)

    def ho_out(j):
        return remote(ho.at[j], hr.at[p0], ho_s.at[j], ho_r.at[p0], j * R + r, t)

    def q_landed(j):
        remote(q.at[j], q.at[j], q_s.at[0, 0], q_r.at[j], s, t).wait_recv()

    @pl.loop(0, P + 1)
    def _(k):
        @pl.when(jnp.logical_and(mine, k < P))
        def _():
            u = flip(p0, k, P)
            src = u * R + r

            @pl.when(k > 0)
            def _():
                landed(src)

            for j in range(1, R):
                to_pair(u, j).start()
            for j in range(1, T):
                to_core(src, j).start()

        @pl.when(k > 0)
        def _():
            u = flip(p0, k - 1, P)

            @pl.when(mine)
            def _():
                for j in range(1, R):
                    src = u * R + (r + j) % R
                    landed(src)
                    for i in range(1, T):
                        to_core(src, i).start()

            @pl.when(jnp.logical_not(mine))
            def _():
                for j in range(R):
                    landed(u * R + (r + j) % R)

            @pl.when(k == 1)
            def _():
                @pl.when(jnp.logical_not(mine))
                def _():
                    q_landed(p0)

                for i in range(1, near):
                    q_landed(flip(p0, i, P))

            turn_values(u)
            attend([flip(p0, i, P) for i in range(near)], u)

    for i in range(near):
        j = flip(p0, i, P)
        finish(j)
        if i == 0:
            hr[p0] = ho[p0]
        else:
            ho_out(j).start()

    size = 2 if (P - near) % 2 == 0 else 1

    @pl.loop(0, (P - near) // size)
    def _(m):
        blocks = [flip(p0, near + m * size + i, P) for i in range(size)]
        for j in blocks:
            q_landed(j)

        @pl.loop(0, P)
        def _(u):
            attend(blocks, u)

        for j in blocks:
            finish(j)
            ho_out(j).start()

    for i in range(1, T):
        from_core(wo, wo_r, i)
    for i in range(1, P):
        o = flip(p0, i, P)
        remote(hr.at[o], hr.at[o], ho_s.at[o], ho_r.at[o], s, t).wait_recv()

    branch = None
    for i in range(T):
        part = jnp.concatenate([hr[i * G + j] for j in range(G)], axis=1)
        term = jnp.dot(part, wo[i], preferred_element_type=F32)
        branch = term if branch is None else branch + term
    out_ref[...] = (lat[t].astype(F32) + modrow[0:1, 2 * D :] * branch).astype(BF16)

    for j in range(1, FB):
        mp_copy(j).wait_send()
    for i in range(1, T):
        lat_copy(i).wait_send()
        lb_copy(i).wait_send()
        wo_copy(i).wait_send()
    for i in range(1, A):
        mod_copy(i, a0).wait_send()

    @pl.when(jnp.logical_not(mine))
    def _():
        kv_out(0).wait_send()
        q_out(0, 0).wait_send()

    for i in range(1, G):
        kv_out(i).wait_send()
    for i in range(G):
        for j in range(T):
            if i + j > 0:
                q_out(i, j).wait_send()
    for i in range(1, P):
        ho_out(flip(p0, i, P)).wait_send()

    @pl.when(mine)
    def _():
        @pl.loop(0, P)
        def _(u):
            for j in range(1, R):
                to_pair(u, j).wait_send()
            for i in range(R):
                for j in range(1, T):
                    to_core(u * R + i, j).wait_send()


def body(
    S, T,
    latent, context, condition, context_condition, modulation_weight,
    query_first, query_second, key_first, key_second, value_weight,
    lambda_head, context_score_boost, head_gain, output_weight,
):
    rows, D = latent.shape
    Lr = rows * T
    G = value_weight.shape[1] // VALUE_DIM
    P = T * G
    assert S % P == 0 and P & (P - 1) == 0 and rows <= LANES
    R = S // P
    B = max(d for d in range(1, S + 1) if S % d == 0 and d * d <= S)
    A = S // B
    Cr = context.shape[0]
    Cp = -(-Cr // 16) * 16
    if Cp != Cr:
        context = jnp.pad(context, ((0, Cp - Cr), (0, 0)))
    cw = modulation_weight.shape[1]
    cp = -(-cw // LANES) * LANES
    if cp != cw:
        modulation_weight = jnp.pad(modulation_weight, ((0, 0), (0, cp - cw)))
    depth = modulation_weight.shape[0]
    assert Lr % GRID_W == 0
    tables = rotation_tables(S * Lr // GRID_W)
    vm = pl.BlockSpec(memory_space=pltpu.VMEM)
    sm = pl.BlockSpec(memory_space=pltpu.SMEM)
    hb = pl.BlockSpec(memory_space=pl.ANY)
    V = pltpu.VMEM
    dma = pltpu.SemaphoreType.DMA
    keys = Lr + Cp
    weights = (query_first, query_second, key_first, key_second, value_weight)
    return pl.pallas_call(
        functools.partial(kernel, (S, T, G, R, A, B, Cr, cw)),
        out_shape=jax.ShapeDtypeStruct((rows, D), BF16),
        in_specs=[hb] * 10 + [sm, sm, vm, hb, vm, vm, vm, vm],
        out_specs=vm,
        scratch_shapes=[V(w.shape, BF16) for w in weights]
        + [
            V((T,) + output_weight.shape, BF16),
            V((Cp, D), BF16),
            V((2, depth), F32),
            V((depth, cp), BF16),
            V((keys, LANES), F32),
            V((keys, LANES), F32),
            V((B * T, 2, cp), F32),
            V((A, B, 2, cp), F32),
            V((2, 3 * D), F32),
            V((T, rows, D), BF16),
            V((keys, D), F32),
            V((keys, D), BF16),
            V((G, Lr, LANES), BF16),
            V((G, keys, LANES + VALUE_DIM), BF16),
            V((P, rows, LANES), BF16),
            V((S, keys, LANES + VALUE_DIM), BF16),
            V((P, VALUE_DIM + 16, R * keys), BF16),
            V((P, 1, 2 * rows), F32),
            V((P, VALUE_DIM + 16, 2 * rows), F32),
            V((P, rows, VALUE_DIM), BF16),
            V((P, rows, VALUE_DIM), BF16),
            V((T, 2 * G, LANES), F32),
            dma((6,)), dma((5,)),
            dma((B * T,)), dma((B * T,)), dma((A,)), dma((A,)),
            dma((T,)), dma((T,)), dma((T,)), dma((T,)), dma((T,)), dma((T,)),
            dma((G, T)), dma((P,)), dma((G,)), dma((S,)), dma((P, R)), dma((S, T)),
            dma((P,)), dma((P,)),
        ],
        compiler_params=pltpu.CompilerParams(
            collective_id=0, has_side_effects=True, vmem_limit_bytes=62 * 1024 * 1024
        ),
    )(
        latent, context, condition[None, :], context_condition[None, :], modulation_weight,
        query_first, query_second, key_first, key_second, value_weight,
        lambda_head, context_score_boost, head_gain[None, :], output_weight, *tables,
    )


def solution(mesh):
    in_specs = (
        P(("sp", "tp"), None),
        P("sp", None),
        P("tp"),
        P("tp"),
        P("tp", "sp"),
        P(None, "tp"),
        P(None, "tp"),
        P(None, "tp"),
        P(None, "tp"),
        P(None, "tp"),
        P("tp"),
        P("tp"),
        P(),
        P("tp", None),
    )
    out_specs = P(("sp", "tp"), None)
    run = functools.partial(body, mesh.shape["sp"], mesh.shape["tp"])
    return jax.shard_map(run, mesh=mesh, in_specs=in_specs, out_specs=out_specs, check_vma=False)
```

time: 64.8 us -> 77.1 us (1.19); the launches traced: 64.6 us -> 75.6 us
  Pallas kernels: 62.7 us -> 73.7 us
    pallas_call x1, Pallas kernels: 62.7 us -> 73.7 us  [body(): pl.pallas_call(functools.partial(kernel, (S, T, G, R, A, B, Cr, cw)), out...]
where the time goes in v1:
time: 77.1 us; the launch traced here: 75.6 us
  Pallas kernels  73.7 us (96%)
  local copies, waits for them, and re-layouts  1.88 us (2%)
    pallas_call x1, Pallas kernels, body(): pl.pallas_call(functools.partial(kernel, (S, T, G, R, A, B, Cr, cw)), out...  73.7 us
    unnamed x1, local copies, waits for them, and re-layouts  1.88 us

profile of v1, /device:TPU:1, one launch (start us, length us, event | category | flops | bytes accessed | tf_op | source)
XLA Modules:
  0.0 75.6 jit_solution(11573309056338308638)
XLA Ops:
  0.0 73.7 %shard_map.172 = bf16[128,2048]{1,0:T(8,128)(2,1)} custom-call(bf16[128,2048]{1,0:T(8,128)(2,1)} %lat_hbm.1, bf16[32,2048]{1,0:T(8,128)(2,1)} %ctx_hbm.1, f32[1,1024]{1,0:T(1,128)} %bitcast.3, f32[1,1024]{1,0:T(1,128)} %bitcast.4, bf16[1024,384]{1,0:T(8,128)(2,1)} %modw_hbm.1, bf16[2048,256]{1,0:T(8,128)(2,1)} %wq1_hbm.1, bf16[2048,256]{1,0:T(8,128)(2,1)} %wq2_hbm.1, ...), custom_call_target="tpu_custom_call" | custom-call | tf_op jit(solution)/shard_map/pallas_call | solution.py:505
  73.7 1.9 %copy.20 = bf16[128,2048]{1,0:T(8,128)(2,1)} copy(bf16[128,2048]{1,0:T(8,128)(2,1)} %shard_map.172) | data formatting | bytes 1048576

commit v2 on v1

v2 whole, which is shorter than its diff:
```python
import functools
import math

import jax
import jax.numpy as jnp
import numpy as np
from jax import lax
from jax.experimental import pallas as pl
from jax.experimental.pallas import tpu as pltpu
from jax.sharding import PartitionSpec as P

HEAD_DIM = 64
VALUE_DIM = 128
GRID_W = 64
EPSILON = 1e-06
THETA = 10000.0
NEGATIVE = -1e30
LOG2E = math.log2(math.e)
MESH = pl.DeviceIdType.MESH
BF16 = jnp.bfloat16
F32 = jnp.float32
LANES = 128


def rotation_tables(grid_rows):
    half = HEAD_DIM // 2
    quarter = half // 2
    lane = np.arange(LANES) % HEAD_DIM
    rate = (THETA ** (-(lane % quarter) / quarter)).astype(np.float32)
    sign = np.where(lane % half < quarter, -1.0, 1.0)
    tables = []
    for count, mask in ((grid_rows, lane < half), (GRID_W, lane >= half)):
        angle = np.arange(count, dtype=np.float32)[:, None] * rate[None, :]
        for table in (np.cos(angle), np.sin(angle) * sign):
            tables.append(np.where(mask, table, 0.0).astype(np.float32))
    return tables


def rotate(x, cosine, sine):
    quarter = HEAD_DIM // 4
    lane = lax.broadcasted_iota(jnp.int32, x.shape, 1)
    ahead = pltpu.roll(x, LANES - quarter, 1)
    behind = pltpu.roll(x, quarter, 1)
    flipped = jnp.where(lane % (2 * quarter) < quarter, ahead, behind)
    return x * cosine + flipped * sine


def normed_rows(rows):
    v = rows.astype(F32)
    return v * lax.rsqrt(jnp.mean(v * v, axis=-1, keepdims=True) + EPSILON)


def flip(v, k, span):
    out = 0
    bit = 1
    while bit < span:
        out = out + bit * ((v // bit + k // bit) % 2)
        bit *= 2
    return out


def kernel(
    dims,
    lat_hbm, ctx_hbm, cond_hbm, ccond_hbm, modw_hbm,
    wq1_hbm, wq2_hbm, wk1_hbm, wk2_hbm, wv_hbm,
    lam_ref, boost_ref, gain_ref, wo_hbm, crow_ref, srow_ref, ccol_ref, scol_ref,
    out_ref,
    wq1, wq2, wk1, wk2, wv, wo,
    ctx, cond, modw, tab, cos_ref, sin_ref, mp, modall, modrow, lat, raw, nrm, h, hraw,
    qs, kvs, kvrs, q, qb, kvn, kvr, kvf, s0, s1, vt0, vt1, pk0, pk1, mx, acc, ho, hr, lb,
    wsem, isem, mp_s, mp_r, ma_s, ma_r, lt_s, lt_r, lb_s, lb_r, wo_s, wo_r,
    rw_s, rw_r, rf_s, rf_r, q_s, q_r, kn_s, kn_r, kf_s, kf_r, kr_s, kr_r, fn_s, ff_s, fr_s, ho_s, ho_r,
):
    S, T, G, R, A, B, Cr, cw = dims
    P = T * G
    s, t = lax.axis_index("sp"), lax.axis_index("tp")
    g, p0 = s // P, s % P
    a0, b0 = s // B, s % B
    prim, hown = p0 // G, p0 % G
    mine = t == prim
    other = jnp.logical_not(mine)
    _, rows, D = lat.shape
    Lr = rows * T
    Cp = ctx.shape[0]
    Q = R - 1
    chunks, rc = raw.shape[2], raw.shape[3]
    rw = chunks * rc
    Rr = T * rw
    N = 2 * P * rows

    def remote(src, dst, send, recv, sp, tp):
        return pltpu.make_async_remote_copy(
            src_ref=src, dst_ref=dst, send_sem=send, recv_sem=recv,
            device_id=(sp, tp), device_id_type=MESH,
        )

    def arrived(buf, recv):
        remote(buf, buf, lt_s.at[0], recv, s, t).wait_recv()

    f0 = b0 * T + t
    FB = B * T

    def plane(j):
        f = (f0 + j) % FB
        return f, a0 * B + f // T, f % T

    barrier = pltpu.get_barrier_semaphore()
    for i in range(1, A):
        pl.semaphore_signal(
            barrier, inc=1, device_id=((a0 + i) % A * B + b0, t), device_id_type=MESH
        )
    for j in range(1, FB):
        _, sp, tp = plane(j)
        pl.semaphore_signal(barrier, inc=1, device_id=(sp, tp), device_id_type=MESH)

    inputs = [
        pltpu.make_async_copy(a, b, isem.at[i])
        for i, (a, b) in enumerate(
            [(cond_hbm, cond.at[0:1]), (ccond_hbm, cond.at[1:2]), (modw_hbm, modw),
             (lat_hbm, lat.at[t]), (ctx_hbm, ctx)]
        )
    ]
    for load in inputs:
        load.start()
    loads = [
        pltpu.make_async_copy(a, b, wsem.at[i])
        for i, (a, b) in enumerate(
            [(wk1_hbm, wk1), (wk2_hbm, wk2), (wv_hbm, wv), (wq1_hbm, wq1), (wq2_hbm, wq2), (wo_hbm, wo.at[t])]
        )
    ]
    for load in loads:
        load.start()

    for i in range(G):
        lb[t, i : i + 1, :] = jnp.full((1, LANES), lam_ref[i], F32)
        lb[t, G + i : G + i + 1, :] = jnp.full((1, LANES), boost_ref[i] * LOG2E, F32)

    for i in range(3):
        inputs[i].wait()
    v = cond[...]
    sig = v / (1.0 + jnp.exp(-v))
    mp[f0] = jnp.dot(sig.astype(BF16), modw[...], preferred_element_type=F32)
    for i in range(3, 5):
        inputs[i].wait()

    pl.semaphore_wait(barrier, FB - 1 + A - 1)

    def mp_copy(j):
        _, sp, tp = plane(j)
        return remote(mp.at[f0], mp.at[f0], mp_s.at[j], mp_r.at[f0], sp, tp)

    def lat_copy(i):
        return remote(lat.at[t], lat.at[t], lt_s.at[i], lt_r.at[t], s, (t + i) % T)

    def lb_copy(i):
        return remote(lb.at[t], lb.at[t], lb_s.at[i], lb_r.at[t], s, (t + i) % T)

    def wo_copy(i):
        return remote(wo.at[t], wo.at[t], wo_s.at[i], wo_r.at[t], s, (t + i) % T)

    def raw_copy(j, c):
        return remote(
            lat.at[t, pl.ds(c * rc, rc)], raw.at[j - 1, t, c], rw_s.at[j - 1, c],
            rw_r.at[j - 1, c], (g + R - j) % R * P + p0, t,
        )

    def raw_pass(j, c, i):
        part = raw.at[j - 1, t, c]
        return remote(
            part, part, rf_s.at[j - 1, c, i], rf_r.at[j - 1, c, t], s, (t + i) % T
        )

    for j in range(1, FB):
        mp_copy(j).start()
    for i in range(1, T):
        lat_copy(i).start()
        lb_copy(i).start()
    for j in range(1, R):
        raw_copy(j, 0).start()

    def table(src, out, order):
        for n, (col, row) in enumerate(((ccol_ref, crow_ref), (scol_ref, srow_ref))):
            for i in range(Lr // GRID_W):
                at = pl.ds(src * (Lr // GRID_W) + i, 1)
                tab[n, i * GRID_W : (i + 1) * GRID_W, :] = col[...] + row[at, :]
            at = out
            for low, high in order:
                ref = sin_ref if n else cos_ref
                ref[at : at + high - low, :] = tab[n, low:high, :]
                at += high - low

    head = [(i * rows, i * rows + rw) for i in range(T)]
    rest = [(i * rows + rw, (i + 1) * rows) for i in range(T)]
    table(s, 0, head + rest)
    cos_ref[Lr : Lr + Cp, :] = jnp.ones((Cp, LANES), F32)
    sin_ref[Lr : Lr + Cp, :] = jnp.zeros((Cp, LANES), F32)
    for j in range(1, R):
        table((g + j) % R * P + p0, Lr + Cp + (j - 1) * Rr, head)

    for j in range(1, FB):
        f, _, _ = plane(j)
        arrived(mp.at[f], mp_r.at[f])
    for b in range(B):
        total = mp[b * T]
        for i in range(1, T):
            total = total + mp[b * T + i]
        modall[a0, b] = total

    def mod_copy(i):
        return remote(
            modall.at[a0], modall.at[a0], ma_s.at[i], ma_r.at[a0], (a0 + i) % A * B + b0, t
        )

    for i in range(1, A):
        mod_copy(i).start()
    for c in range(1, chunks):
        for j in range(1, R):
            raw_copy(j, c).start()

    step = math.gcd(rw, rows - rw, 32)

    def norm_lat(i):
        for low, size, at in ((0, rw, i * rw), (rw, rows - rw, Rr + i * (rows - rw))):

            @pl.loop(0, size // step)
            def _(j):
                off = pl.multiple_of(j * step, step)
                to = pl.ds(pl.multiple_of(at + off, step), step)
                nrm[to, :] = normed_rows(lat[i, pl.ds(low + off, step), :])

    nrm[Lr:, :] = normed_rows(ctx[...])
    norm_lat(t)
    for i in range(1, T):
        o = (t + i) % T
        arrived(lat.at[o], lt_r.at[o])
        norm_lat(o)

    for i in range(1, A):
        o = (a0 + i) % A
        arrived(modall.at[o], ma_r.at[o])
    for a in range(A):
        for b in range(B):
            i = a * B + b
            modrow[:, i * cw : (i + 1) * cw] = modall[a, b][:, :cw]

    @pl.loop(0, Lr // step)
    def _(j):
        at = pl.ds(pl.multiple_of(j * step, step), step)
        h[at, :] = (nrm[at, :] * (1.0 + modrow[0:1, D : 2 * D]) + modrow[0:1, :D]).astype(BF16)

    h[Lr:, :] = (nrm[Lr:, :] * (1.0 + modrow[1:2, D : 2 * D]) + modrow[1:2, :D]).astype(BF16)

    def project(hh, at, out):
        n = hh.shape[0]
        one = jnp.dot(hh, wk1[...], preferred_element_type=F32)
        two = jnp.dot(hh, wk2[...], preferred_element_type=F32)
        for i in range(G):
            cut = slice(i * HEAD_DIM, (i + 1) * HEAD_DIM)
            pair = jnp.concatenate([one[:, cut], two[:, cut]], axis=1)
            turned = rotate(pair, cos_ref[at : at + n, :], sin_ref[at : at + n, :])
            out[i, :, :LANES] = turned.astype(BF16)
        val = jnp.dot(hh, wv[...], preferred_element_type=F32)
        for i in range(G):
            out[i, :, LANES:] = val[:, i * VALUE_DIM : (i + 1) * VALUE_DIM].astype(BF16)

    for i in range(3):
        loads[i].wait()
    project(h[...], 0, kvs)

    def near_out(i):
        hl = flip(hown, i, G)
        return remote(kvs.at[hl], kvn.at[p0], kn_s.at[i], kn_r.at[p0], g * P + t * G + hl, t)

    def far_out(i, j):
        hl = flip(hown, i, G)
        to = (g + R - j) % R
        slot = (j - 1) * P + p0
        return remote(
            kvs.at[hl, pl.ds(Rr, Lr + Cp - Rr)], kvf.at[slot], kf_s.at[i, j - 1], kf_r.at[slot],
            to * P + t * G + hl, t,
        )

    def raw_out(i):
        hl = flip(hown, i, G)
        return remote(kvrs.at[hl], kvr.at[p0], kr_s.at[i], kr_r.at[p0], g * P + t * G + hl, t)

    @pl.when(mine)
    def _():
        kvn[p0] = kvs[hown]

    @pl.when(other)
    def _():
        near_out(0).start()

    for i in range(1, G):
        near_out(i).start()

    for i in range(3, 5):
        loads[i].wait()
    lh = h[:Lr, :]
    one = jnp.dot(lh, wq1[...], preferred_element_type=F32)
    two = jnp.dot(lh, wq2[...], preferred_element_type=F32)
    for i in range(G):
        cut = slice(i * HEAD_DIM, (i + 1) * HEAD_DIM)
        pair = jnp.concatenate([one[:, cut], two[:, cut]], axis=1)
        turned = rotate(pair, cos_ref[:Lr, :], sin_ref[:Lr, :])
        turned = (turned * (LOG2E * HEAD_DIM**-0.5)).astype(BF16)
        at = 0
        for low, high in head + rest:
            qs[i, low:high, :] = turned[at : at + high - low]
            at += high - low

    def q_out(i, j):
        hl = flip(hown, i, G)
        to = (t + j) % T
        part = pl.ds(pl.multiple_of(to * rows, rows), rows)
        return remote(qs.at[hl, part], q.at[p0], q_s.at[i, j], q_r.at[p0], g * P + t * G + hl, to)

    @pl.when(mine)
    def _():
        q[p0] = qs[hown, pl.ds(pl.multiple_of(t * rows, rows), rows), :]

    @pl.when(other)
    def _():
        q_out(0, 0).start()

    for j in range(1, T):
        q_out(0, j).start()
    for i in range(1, G):
        for j in range(T):
            q_out(i, j).start()
    for i in range(G):
        for j in range(1, R):
            far_out(i, j).start()

    for c in range(chunks):
        for j in range(1, R):
            arrived(raw.at[j - 1, t, c], rw_r.at[j - 1, c])
            for i in range(1, T):
                raw_pass(j, c, i).start()

    def lift(j, o, c):
        part = normed_rows(raw[j - 1, o, c])
        part = part * (1.0 + modrow[0:1, D : 2 * D]) + modrow[0:1, :D]
        at = pl.multiple_of((j - 1) * Rr + o * rw + c * rc, rc)
        hraw[pl.ds(at, rc), :] = part.astype(BF16)

    for j in range(1, R):
        for c in range(chunks):
            lift(j, t, c)
    for i in range(1, T):
        o = (t + i) % T
        for c in range(chunks):
            for j in range(1, R):
                arrived(raw.at[j - 1, o, c], rf_r.at[j - 1, c, o])
                lift(j, o, c)
    project(hraw[...], Lr + Cp, kvrs)

    @pl.when(mine)
    def _():
        kvr[p0] = kvrs[hown]

    @pl.when(other)
    def _():
        raw_out(0).start()

    for i in range(1, G):
        raw_out(i).start()

    loads[5].wait()
    for i in range(1, T):
        wo_copy(i).start()

    mx[...] = jnp.full(mx.shape, NEGATIVE, F32)
    acc[...] = jnp.zeros(acc.shape, F32)
    for vt in (vt0, vt1):
        vt[VALUE_DIM:, :] = jnp.ones((vt.shape[0] - VALUE_DIM, vt.shape[1]), BF16)
    for i in range(1, T):
        o = (t + i) % T
        arrived(lb.at[o], lb_r.at[o])
    lam = lb[prim, pl.ds(hown, 1), :][:, :rows]
    boost = lb[prim, pl.ds(G + hown, 1), :][:, :1]
    gain = jnp.broadcast_to(gain_ref[...], (VALUE_DIM, LANES)).T[:, :rows]
    nt = (((1,), (1,)), ((), ()))

    def to_core(buf, slot, send, recv, i):
        return remote(
            buf.at[slot], buf.at[slot], send.at[slot, i], recv.at[slot], s, (t + i) % T
        )

    def fetch(buf, slots, send, recv, own):
        @pl.when(mine)
        def _():
            for n, slot in enumerate(slots):
                if own:

                    @pl.when(slot != p0)
                    def _():
                        arrived(buf.at[slot], recv.at[slot])

                else:
                    arrived(buf.at[slot], recv.at[slot])
                for i in range(1, T):
                    to_core(buf, slot, send, recv, i).start()

        @pl.when(other)
        def _():
            for slot in slots:
                arrived(buf.at[slot], recv.at[slot])

    def scores(buf, base, count, low, s_ref, vt_ref, pk_ref):
        span = buf.shape[1]
        at = pl.ds(base, count)
        keys = buf[at, :low, :LANES].reshape(count * low, LANES)
        vals = buf[at, :low, LANES:].reshape(count * low, VALUE_DIM)
        sc = lax.dot_general(keys, qb[...], nt, preferred_element_type=F32)
        n = count * low
        s_ref[:n, :] = sc
        peak = jnp.max(sc, axis=0, keepdims=True)
        vt_ref[:VALUE_DIM, :n] = vals.astype(F32).T.astype(BF16)
        if span > low:
            m = count * (span - low)
            keys = buf[at, low:, :LANES].reshape(m, LANES)
            vals = buf[at, low:, LANES:].reshape(m, VALUE_DIM)
            sc = lax.dot_general(keys, qb[...], nt, preferred_element_type=F32) + boost
            if Cp != Cr:
                spot = lax.broadcasted_iota(jnp.int32, sc.shape, 0)
                sc = jnp.where(spot % Cp < Cr, sc, NEGATIVE)
            s_ref[n : n + m, :] = sc
            peak = jnp.maximum(peak, jnp.max(sc, axis=0, keepdims=True))
            vt_ref[:VALUE_DIM, n : n + m] = vals.astype(F32).T.astype(BF16)
        pk_ref[...] = peak

    def weigh(n, s_ref, vt_ref, pk_ref):
        old = mx[...]
        peak = jnp.maximum(old, pk_ref[...])
        pr = jnp.exp2(s_ref[:n, :] - peak).astype(BF16)
        mx[...] = peak
        acc[...] = jnp.exp2(old - peak) * acc[...] + jnp.dot(
            vt_ref[:, :n], pr, preferred_element_type=F32
        )

    def finish(j):
        u = acc[:VALUE_DIM, j * 2 * rows : (j + 1) * 2 * rows]
        u = u / acc[VALUE_DIM : VALUE_DIM + 1, j * 2 * rows : (j + 1) * 2 * rows]
        mixed = u[:, :rows] - lam * u[:, rows:]
        mixed = mixed * lax.rsqrt(jnp.mean(mixed * mixed, axis=0, keepdims=True) + EPSILON)
        ho[j] = (mixed * gain).T.astype(BF16)

    def ho_out(j):
        return remote(ho.at[j], hr.at[p0], ho_s.at[j], ho_r.at[p0], g * P + j, t)

    for j in range(P):

        @pl.when(jnp.logical_or(other, p0 != j))
        def _():
            arrived(q.at[j], q_r.at[j])

        qq = q[j]
        lane = lax.broadcasted_iota(jnp.int32, qq.shape, 1)
        zero = jnp.zeros_like(qq)
        qb[j * 2 * rows : j * 2 * rows + rows, :] = jnp.where(lane < HEAD_DIM, qq, zero)
        qb[j * 2 * rows + rows : (j + 1) * 2 * rows, :] = jnp.where(lane < HEAD_DIM, zero, qq)

    units = []
    pair = min(2, P)
    for k in range(P // pair):
        units.append((kvn, flip(p0 // pair, k, P // pair) * pair, pair, Lr, fn_s, kn_r, True))
    quad = math.gcd(P, max(1, 640 // (Q * Rr)))
    for k in range(P // quad):
        units.append((kvr, flip(p0 // quad, k, P // quad) * quad, quad, Q * Rr, fr_s, kr_r, True))
    wide = math.gcd(P, max(1, 640 // kvf.shape[1]))
    for j in range(Q):
        for k in range(P // wide):
            base = j * P + flip(p0 // wide, k, P // wide) * wide
            units.append((kvf, base, wide, Lr - Rr, ff_s, kf_r, False))
    banks = ((s0, vt0, pk0), (s1, vt1, pk1))
    last = None
    for n, (buf, base, count, low, send, recv, own) in enumerate(units):
        fetch(buf, [base + i for i in range(count)], send, recv, own)
        scores(buf, base, count, low, *banks[n % 2])
        if last is not None:
            weigh(last, *banks[(n - 1) % 2])
        last = count * buf.shape[1]
    weigh(last, *banks[(len(units) - 1) % 2])

    for j in range(P):
        finish(j)

        @pl.when(p0 == j)
        def _():
            hr[j] = ho[j]

        @pl.when(p0 != j)
        def _():
            ho_out(j).start()

    for i in range(1, T):
        o = (t + i) % T
        arrived(wo.at[o], wo_r.at[o])
    for i in range(1, P):
        o = flip(p0, i, P)
        arrived(hr.at[o], ho_r.at[o])

    branch = None
    for i in range(T):
        part = jnp.concatenate([hr[i * G + j] for j in range(G)], axis=1)
        term = jnp.dot(part, wo[i], preferred_element_type=F32)
        branch = term if branch is None else branch + term
    out_ref[...] = (lat[t].astype(F32) + modrow[0:1, 2 * D :] * branch).astype(BF16)

    for j in range(1, FB):
        mp_copy(j).wait_send()
    for i in range(1, T):
        lat_copy(i).wait_send()
        lb_copy(i).wait_send()
        wo_copy(i).wait_send()
    for i in range(1, A):
        mod_copy(i).wait_send()
    for j in range(1, R):
        for c in range(chunks):
            raw_copy(j, c).wait_send()
            for i in range(1, T):
                raw_pass(j, c, i).wait_send()

    @pl.when(other)
    def _():
        near_out(0).wait_send()
        raw_out(0).wait_send()
        q_out(0, 0).wait_send()

    for i in range(1, G):
        near_out(i).wait_send()
        raw_out(i).wait_send()
    for i in range(G):
        for j in range(1, R):
            far_out(i, j).wait_send()
        for j in range(T):
            if i + j > 0:
                q_out(i, j).wait_send()
    for i in range(1, P):
        ho_out(flip(p0, i, P)).wait_send()

    @pl.when(mine)
    def _():
        for buf, send, recv in ((kvn, fn_s, kn_r), (kvr, fr_s, kr_r), (kvf, ff_s, kf_r)):

            @pl.loop(0, buf.shape[0])
            def _(slot):
                for i in range(1, T):
                    to_core(buf, slot, send, recv, i).wait_send()


def body(
    S, T,
    latent, context, condition, context_condition, modulation_weight,
    query_first, query_second, key_first, key_second, value_weight,
    lambda_head, context_score_boost, head_gain, output_weight,
):
    rows, D = latent.shape
    Lr = rows * T
    G = value_weight.shape[1] // VALUE_DIM
    P = T * G
    assert S % P == 0 and P & (P - 1) == 0 and rows <= LANES
    R = S // P
    B = max(d for d in range(1, S + 1) if S % d == 0 and d * d <= S)
    A = S // B
    assert R > 1 and P % B == 0
    rc = 16
    chunks = rows * 5 // 8 // rc
    Rr = T * chunks * rc
    Cr = context.shape[0]
    Cp = -(-Cr // 16) * 16
    if Cp != Cr:
        context = jnp.pad(context, ((0, Cp - Cr), (0, 0)))
    cw = modulation_weight.shape[1]
    cp = -(-cw // LANES) * LANES
    if cp != cw:
        modulation_weight = jnp.pad(modulation_weight, ((0, 0), (0, cp - cw)))
    depth = modulation_weight.shape[0]
    assert Lr % GRID_W == 0
    tables = rotation_tables(S * Lr // GRID_W)
    vm = pl.BlockSpec(memory_space=pltpu.VMEM)
    sm = pl.BlockSpec(memory_space=pltpu.SMEM)
    hb = pl.BlockSpec(memory_space=pl.ANY)
    V = pltpu.VMEM
    dma = pltpu.SemaphoreType.DMA
    keys = Lr + Cp
    Q = R - 1
    N = 2 * P * rows
    pairw = LANES + VALUE_DIM
    most = max(2 * keys, Q * Rr, 640)
    weights = (query_first, query_second, key_first, key_second, value_weight)
    return pl.pallas_call(
        functools.partial(kernel, (S, T, G, R, A, B, Cr, cw)),
        out_shape=jax.ShapeDtypeStruct((rows, D), BF16),
        in_specs=[hb] * 10 + [sm, sm, vm, hb, vm, vm, vm, vm],
        out_specs=vm,
        scratch_shapes=[V(w.shape, BF16) for w in weights]
        + [
            V((T,) + output_weight.shape, BF16),
            V((Cp, D), BF16),
            V((2, depth), F32),
            V((depth, cp), BF16),
            V((2, Lr, LANES), F32),
            V((keys + Q * Rr, LANES), F32),
            V((keys + Q * Rr, LANES), F32),
            V((B * T, 2, cp), F32),
            V((A, B, 2, cp), F32),
            V((2, 3 * D), F32),
            V((T, rows, D), BF16),
            V((Q, T, chunks, rc, D), BF16),
            V((keys, D), F32),
            V((keys, D), BF16),
            V((Q * Rr, D), BF16),
            V((G, Lr, LANES), BF16),
            V((G, keys, pairw), BF16),
            V((G, Q * Rr, pairw), BF16),
            V((P, rows, LANES), BF16),
            V((N, LANES), BF16),
            V((P, keys, pairw), BF16),
            V((P, Q * Rr, pairw), BF16),
            V((Q * P, keys - Rr, pairw), BF16),
            V((most, N), F32),
            V((most, N), F32),
            V((VALUE_DIM + 16, most), BF16),
            V((VALUE_DIM + 16, most), BF16),
            V((1, N), F32),
            V((1, N), F32),
            V((1, N), F32),
            V((VALUE_DIM + 16, N), F32),
            V((P, rows, VALUE_DIM), BF16),
            V((P, rows, VALUE_DIM), BF16),
            V((T, 2 * G, LANES), F32),
            dma((6,)), dma((5,)),
            dma((B * T,)), dma((B * T,)), dma((A,)), dma((A,)),
            dma((T,)), dma((T,)), dma((T,)), dma((T,)), dma((T,)), dma((T,)),
            dma((Q, chunks)), dma((Q, chunks)), dma((Q, chunks, T)), dma((Q, chunks, T)),
            dma((G, T)), dma((P,)),
            dma((G,)), dma((P,)), dma((G, Q)), dma((Q * P,)), dma((G,)), dma((P,)),
            dma((P, T)), dma((Q * P, T)), dma((P, T)),
            dma((P,)), dma((P,)),
        ],
        compiler_params=pltpu.CompilerParams(
            collective_id=0, has_side_effects=True, vmem_limit_bytes=62 * 1024 * 1024
        ),
    )(
        latent, context, condition[None, :], context_condition[None, :], modulation_weight,
        query_first, query_second, key_first, key_second, value_weight,
        lambda_head, context_score_boost, head_gain[None, :], output_weight, *tables,
    )


def solution(mesh):
    in_specs = (
        P(("sp", "tp"), None),
        P("sp", None),
        P("tp"),
        P("tp"),
        P("tp", "sp"),
        P(None, "tp"),
        P(None, "tp"),
        P(None, "tp"),
        P(None, "tp"),
        P(None, "tp"),
        P("tp"),
        P("tp"),
        P(),
        P("tp", None),
    )
    out_specs = P(("sp", "tp"), None)
    run = functools.partial(body, mesh.shape["sp"], mesh.shape["tp"])
    return jax.shard_map(run, mesh=mesh, in_specs=in_specs, out_specs=out_specs, check_vma=False)
```

time: 77.1 us -> 65.9 us (0.85)
  Pallas kernels: 73.7 us -> 63.1 us
    pallas_call x1, Pallas kernels: 73.7 us -> 63.1 us  [body(): pl.pallas_call(functools.partial(kernel, (S, T, G, R, A, B, Cr, cw)), out...]
where the time goes in v2:
time: 65.9 us; the launch traced here: 65 us
  Pallas kernels  63.1 us (96%)
  local copies, waits for them, and re-layouts  1.88 us (3%)
    pallas_call x1, Pallas kernels, body(): pl.pallas_call(functools.partial(kernel, (S, T, G, R, A, B, Cr, cw)), out...  63.1 us
    unnamed x1, local copies, waits for them, and re-layouts  1.88 us

profile of v2, /device:TPU:1, one launch (start us, length us, event | category | flops | bytes accessed | tf_op | source)
XLA Modules:
  0.0 65.0 jit_solution(16362506357567775242)
XLA Ops:
  0.0 63.1 %shard_map.172 = bf16[128,2048]{1,0:T(8,128)(2,1)} custom-call(bf16[128,2048]{1,0:T(8,128)(2,1)} %lat_hbm.1, bf16[32,2048]{1,0:T(8,128)(2,1)} %ctx_hbm.1, f32[1,1024]{1,0:T(1,128)} %bitcast.3, f32[1,1024]{1,0:T(1,128)} %bitcast.4, bf16[1024,384]{1,0:T(8,128)(2,1)} %modw_hbm.1, bf16[2048,256]{1,0:T(8,128)(2,1)} %wq1_hbm.1, bf16[2048,256]{1,0:T(8,128)(2,1)} %wq2_hbm.1, ...), custom_call_target="tpu_custom_call" | custom-call | tf_op jit(solution)/shard_map/pallas_call | solution.py:594
  63.1 1.9 %copy.20 = bf16[128,2048]{1,0:T(8,128)(2,1)} copy(bf16[128,2048]{1,0:T(8,128)(2,1)} %shard_map.172) | data formatting | bytes 1048576

commit v3 on v2

--- a/solution.py
+++ b/solution.py
@@ -20,6 +20,7 @@
 BF16 = jnp.bfloat16
 F32 = jnp.float32
 LANES = 128
+QROWS = 256
 
 
 def rotation_tables(grid_rows):
@@ -59,6 +60,10 @@
     return out
 
 
+def groups(P, raw_rows, far_rows):
+    return math.gcd(P, max(1, 400 // raw_rows)), math.gcd(P, max(1, 512 // far_rows))
+
+
 def kernel(
     dims,
     lat_hbm, ctx_hbm, cond_hbm, ccond_hbm, modw_hbm,
@@ -66,27 +71,28 @@
     lam_ref, boost_ref, gain_ref, wo_hbm, crow_ref, srow_ref, ccol_ref, scol_ref,
     out_ref,
     wq1, wq2, wk1, wk2, wv, wo,
-    ctx, cond, modw, tab, cos_ref, sin_ref, mp, modall, modrow, lat, raw, nrm, h, hraw,
+    ctx, cond, modw, tab, cos_ref, sin_ref, mp, modrow, lat, raw, nrm, h, hraw,
     qs, kvs, kvrs, q, qb, kvn, kvr, kvf, s0, s1, vt0, vt1, pk0, pk1, mx, acc, ho, hr, lb,
-    wsem, isem, mp_s, mp_r, ma_s, ma_r, lt_s, lt_r, lb_s, lb_r, wo_s, wo_r,
+    wsem, isem, mp_s, mp_r, lt_s, lt_r, lb_s, lb_r, wo_s, wo_r,
     rw_s, rw_r, rf_s, rf_r, q_s, q_r, kn_s, kn_r, kf_s, kf_r, kr_s, kr_r, fn_s, ff_s, fr_s, ho_s, ho_r,
 ):
-    S, T, G, R, A, B, Cr, cw = dims
+    S, T, G, R, Cr, cw = dims
     P = T * G
     s, t = lax.axis_index("sp"), lax.axis_index("tp")
     g, p0 = s // P, s % P
-    a0, b0 = s // B, s % B
     prim, hown = p0 // G, p0 % G
     mine = t == prim
     other = jnp.logical_not(mine)
     _, rows, D = lat.shape
     Lr = rows * T
     Cp = ctx.shape[0]
+    keys = Lr + Cp
     Q = R - 1
     chunks, rc = raw.shape[2], raw.shape[3]
     rw = chunks * rc
     Rr = T * rw
     N = 2 * P * rows
+    quad, wide = groups(P, Q * Rr, keys - Rr)
 
     def remote(src, dst, send, recv, sp, tp):
         return pltpu.make_async_remote_copy(
@@ -97,21 +103,14 @@
     def arrived(buf, recv):
         remote(buf, buf, lt_s.at[0], recv, s, t).wait_recv()
 
-    f0 = b0 * T + t
-    FB = B * T
-
-    def plane(j):
-        f = (f0 + j) % FB
-        return f, a0 * B + f // T, f % T
-
+    f0 = s * T + t
+    F = S * T
     barrier = pltpu.get_barrier_semaphore()
-    for i in range(1, A):
-        pl.semaphore_signal(
-            barrier, inc=1, device_id=((a0 + i) % A * B + b0, t), device_id_type=MESH
-        )
-    for j in range(1, FB):
-        _, sp, tp = plane(j)
-        pl.semaphore_signal(barrier, inc=1, device_id=(sp, tp), device_id_type=MESH)
+
+    @pl.loop(1, F)
+    def _(i):
+        f = (f0 + i) % F
+        pl.semaphore_signal(barrier, inc=1, device_id=(f // T, f % T), device_id_type=MESH)
 
     inputs = [
         pltpu.make_async_copy(a, b, isem.at[i])
@@ -143,11 +142,11 @@
     for i in range(3, 5):
         inputs[i].wait()
 
-    pl.semaphore_wait(barrier, FB - 1 + A - 1)
-
-    def mp_copy(j):
-        _, sp, tp = plane(j)
-        return remote(mp.at[f0], mp.at[f0], mp_s.at[j], mp_r.at[f0], sp, tp)
+    pl.semaphore_wait(barrier, F - 1)
+
+    def mp_copy(i):
+        f = (f0 + i) % F
+        return remote(mp.at[f0], mp.at[f0], mp_s.at[i], mp_r.at[f0], f // T, f % T)
 
     def lat_copy(i):
         return remote(lat.at[t], lat.at[t], lt_s.at[i], lt_r.at[t], s, (t + i) % T)
@@ -170,13 +169,19 @@
             part, part, rf_s.at[j - 1, c, i], rf_r.at[j - 1, c, t], s, (t + i) % T
         )
 
-    for j in range(1, FB):
-        mp_copy(j).start()
+    @pl.loop(1, F)
+    def _(i):
+        mp_copy(i).start()
+
     for i in range(1, T):
         lat_copy(i).start()
         lb_copy(i).start()
-    for j in range(1, R):
-        raw_copy(j, 0).start()
+    for c in range(chunks):
+        for j in range(1, R):
+            raw_copy(j, c).start()
+    loads[5].wait()
+    for i in range(1, T):
+        wo_copy(i).start()
 
     def table(src, out, order):
         for n, (col, row) in enumerate(((ccol_ref, crow_ref), (scol_ref, srow_ref))):
@@ -197,26 +202,6 @@
     for j in range(1, R):
         table((g + j) % R * P + p0, Lr + Cp + (j - 1) * Rr, head)
 
-    for j in range(1, FB):
-        f, _, _ = plane(j)
-        arrived(mp.at[f], mp_r.at[f])
-    for b in range(B):
-        total = mp[b * T]
-        for i in range(1, T):
-            total = total + mp[b * T + i]
-        modall[a0, b] = total
-
-    def mod_copy(i):
-        return remote(
-            modall.at[a0], modall.at[a0], ma_s.at[i], ma_r.at[a0], (a0 + i) % A * B + b0, t
-        )
-
-    for i in range(1, A):
-        mod_copy(i).start()
-    for c in range(1, chunks):
-        for j in range(1, R):
-            raw_copy(j, c).start()
-
     step = math.gcd(rw, rows - rw, 32)
 
     def norm_lat(i):
@@ -235,13 +220,16 @@
         arrived(lat.at[o], lt_r.at[o])
         norm_lat(o)
 
-    for i in range(1, A):
-        o = (a0 + i) % A
-        arrived(modall.at[o], ma_r.at[o])
-    for a in range(A):
-        for b in range(B):
-            i = a * B + b
-            modrow[:, i * cw : (i + 1) * cw] = modall[a, b][:, :cw]
+    @pl.loop(1, F)
+    def _(i):
+        f = (f0 + i) % F
+        arrived(mp.at[f], mp_r.at[f])
+
+    for i in range(S):
+        total = mp[i * T]
+        for j in range(1, T):
+            total = total + mp[i * T + j]
+        modrow[:, i * cw : (i + 1) * cw] = total[:, :cw]
 
     @pl.loop(0, Lr // step)
     def _(j):
@@ -262,38 +250,6 @@
         val = jnp.dot(hh, wv[...], preferred_element_type=F32)
         for i in range(G):
             out[i, :, LANES:] = val[:, i * VALUE_DIM : (i + 1) * VALUE_DIM].astype(BF16)
-
-    for i in range(3):
-        loads[i].wait()
-    project(h[...], 0, kvs)
-
-    def near_out(i):
-        hl = flip(hown, i, G)
-        return remote(kvs.at[hl], kvn.at[p0], kn_s.at[i], kn_r.at[p0], g * P + t * G + hl, t)
-
-    def far_out(i, j):
-        hl = flip(hown, i, G)
-        to = (g + R - j) % R
-        slot = (j - 1) * P + p0
-        return remote(
-            kvs.at[hl, pl.ds(Rr, Lr + Cp - Rr)], kvf.at[slot], kf_s.at[i, j - 1], kf_r.at[slot],
-            to * P + t * G + hl, t,
-        )
-
-    def raw_out(i):
-        hl = flip(hown, i, G)
-        return remote(kvrs.at[hl], kvr.at[p0], kr_s.at[i], kr_r.at[p0], g * P + t * G + hl, t)
-
-    @pl.when(mine)
-    def _():
-        kvn[p0] = kvs[hown]
-
-    @pl.when(other)
-    def _():
-        near_out(0).start()
-
-    for i in range(1, G):
-        near_out(i).start()
 
     for i in range(3, 5):
         loads[i].wait()
@@ -329,9 +285,41 @@
     for i in range(1, G):
         for j in range(T):
             q_out(i, j).start()
+    for i in range(3):
+        loads[i].wait()
+    project(h[...], 0, kvs)
+
+    def near_out(i):
+        hl = flip(hown, i, G)
+        return remote(kvs.at[hl], kvn.at[p0], kn_s.at[i], kn_r.at[p0], g * P + t * G + hl, t)
+
+    def far_out(i, j):
+        hl = flip(hown, i, G)
+        to = (g + R - j) % R
+        slot = (j - 1) * P + p0
+        return remote(
+            kvs.at[hl, pl.ds(Rr, Lr + Cp - Rr)], kvf.at[slot], kf_s.at[i, j - 1], kf_r.at[slot],
+            to * P + t * G + hl, t,
+        )
+
+    def raw_out(i):
+        hl = flip(hown, i, G)
+        return remote(kvrs.at[hl], kvr.at[p0], kr_s.at[i], kr_r.at[p0], g * P + t * G + hl, t)
+
+    @pl.when(mine)
+    def _():
+        kvn[p0] = kvs[hown]
+
+    @pl.when(other)
+    def _():
+        near_out(0).start()
+
+    for i in range(1, G):
+        near_out(i).start()
     for i in range(G):
         for j in range(1, R):
             far_out(i, j).start()
+
 
     for c in range(chunks):
         for j in range(1, R):
@@ -367,10 +355,6 @@
     for i in range(1, G):
         raw_out(i).start()
 
-    loads[5].wait()
-    for i in range(1, T):
-        wo_copy(i).start()
-
     mx[...] = jnp.full(mx.shape, NEGATIVE, F32)
     acc[...] = jnp.zeros(acc.shape, F32)
     for vt in (vt0, vt1):
@@ -388,10 +372,10 @@
             buf.at[slot], buf.at[slot], send.at[slot, i], recv.at[slot], s, (t + i) % T
         )
 
-    def fetch(buf, slots, send, recv, own):
+    def spread(buf, slots, send, recv, own):
         @pl.when(mine)
         def _():
-            for n, slot in enumerate(slots):
+            for slot in slots:
                 if own:
 
                     @pl.when(slot != p0)
@@ -403,6 +387,7 @@
                 for i in range(1, T):
                     to_core(buf, slot, send, recv, i).start()
 
+    def settle(buf, slots, recv):
         @pl.when(other)
         def _():
             for slot in slots:
@@ -463,21 +448,19 @@
         qb[j * 2 * rows + rows : (j + 1) * 2 * rows, :] = jnp.where(lane < HEAD_DIM, zero, qq)
 
     units = []
-    pair = min(2, P)
-    for k in range(P // pair):
-        units.append((kvn, flip(p0 // pair, k, P // pair) * pair, pair, Lr, fn_s, kn_r, True))
-    quad = math.gcd(P, max(1, 640 // (Q * Rr)))
-    for k in range(P // quad):
-        units.append((kvr, flip(p0 // quad, k, P // quad) * quad, quad, Q * Rr, fr_s, kr_r, True))
-    wide = math.gcd(P, max(1, 640 // kvf.shape[1]))
+    for k in [*range(0, P // 2, 2), *range(1, P // 2, 2)]:
+        units.append((kvn, flip(p0 // 2, k, P // 2) * 2, 2, Lr, fn_s, kn_r, True))
     for j in range(Q):
         for k in range(P // wide):
             base = j * P + flip(p0 // wide, k, P // wide) * wide
             units.append((kvf, base, wide, Lr - Rr, ff_s, kf_r, False))
+    for k in range(P // quad):
+        units.append((kvr, flip(p0 // quad, k, P // quad) * quad, quad, Q * Rr, fr_s, kr_r, True))
     banks = ((s0, vt0, pk0), (s1, vt1, pk1))
     last = None
     for n, (buf, base, count, low, send, recv, own) in enumerate(units):
-        fetch(buf, [base + i for i in range(count)], send, recv, own)
+        spread(buf, [base + i for i in range(count)], send, recv, own)
+        settle(buf, [base + i for i in range(count)], recv)
         scores(buf, base, count, low, *banks[n % 2])
         if last is not None:
             weigh(last, *banks[(n - 1) % 2])
@@ -509,14 +492,14 @@
         branch = term if branch is None else branch + term
     out_ref[...] = (lat[t].astype(F32) + modrow[0:1, 2 * D :] * branch).astype(BF16)
 
-    for j in range(1, FB):
-        mp_copy(j).wait_send()
+    @pl.loop(1, F)
+    def _(i):
+        mp_copy(i).wait_send()
+
     for i in range(1, T):
         lat_copy(i).wait_send()
         lb_copy(i).wait_send()
         wo_copy(i).wait_send()
-    for i in range(1, A):
-        mod_copy(i).wait_send()
     for j in range(1, R):
         for c in range(chunks):
             raw_copy(j, c).wait_send()
@@ -563,11 +546,9 @@
     P = T * G
     assert S % P == 0 and P & (P - 1) == 0 and rows <= LANES
     R = S // P
-    B = max(d for d in range(1, S + 1) if S % d == 0 and d * d <= S)
-    A = S // B
-    assert R > 1 and P % B == 0
+    assert R > 1 and P > 1
     rc = 16
-    chunks = rows * 5 // 8 // rc
+    chunks = rows * 3 // 8 // rc
     Rr = T * chunks * rc
     Cr = context.shape[0]
     Cp = -(-Cr // 16) * 16
@@ -589,10 +570,11 @@
     Q = R - 1
     N = 2 * P * rows
     pairw = LANES + VALUE_DIM
-    most = max(2 * keys, Q * Rr, 640)
+    quad, wide = groups(P, Q * Rr, keys - Rr)
+    most = max(2 * keys, quad * Q * Rr, wide * (keys - Rr))
     weights = (query_first, query_second, key_first, key_second, value_weight)
     return pl.pallas_call(
-        functools.partial(kernel, (S, T, G, R, A, B, Cr, cw)),
+        functools.partial(kernel, (S, T, G, R, Cr, cw)),
         out_shape=jax.ShapeDtypeStruct((rows, D), BF16),
         in_specs=[hb] * 10 + [sm, sm, vm, hb, vm, vm, vm, vm],
         out_specs=vm,
@@ -605,8 +587,7 @@
             V((2, Lr, LANES), F32),
             V((keys + Q * Rr, LANES), F32),
             V((keys + Q * Rr, LANES), F32),
-            V((B * T, 2, cp), F32),
-            V((A, B, 2, cp), F32),
+            V((S * T, 2, cp), F32),
             V((2, 3 * D), F32),
             V((T, rows, D), BF16),
             V((Q, T, chunks, rc, D), BF16),
@@ -633,13 +614,390 @@
             V((P, rows, VALUE_DIM), BF16),
             V((T, 2 * G, LANES), F32),
             dma((6,)), dma((5,)),
-            dma((B * T,)), dma((B * T,)), dma((A,)), dma((A,)),
+            dma((S * T,)), dma((S * T,)),
             dma((T,)), dma((T,)), dma((T,)), dma((T,)), dma((T,)), dma((T,)),
             dma((Q, chunks)), dma((Q, chunks)), dma((Q, chunks, T)), dma((Q, chunks, T)),
             dma((G, T)), dma((P,)),
             dma((G,)), dma((P,)), dma((G, Q)), dma((Q * P,)), dma((G,)), dma((P,)),
             dma((P, T)), dma((Q * P, T)), dma((P, T)),
             dma((P,)), dma((P,)),
+        ],
+        compiler_params=pltpu.CompilerParams(
+            collective_id=0, has_side_effects=True, vmem_limit_bytes=62 * 1024 * 1024
+        ),
+    )(
+        latent, context, condition[None, :], context_condition[None, :], modulation_weight,
+        query_first, query_second, key_first, key_second, value_weight,
+        lambda_head, context_score_boost, head_gain[None, :], output_weight, *tables,
+    )
+
+
+def general_kernel(
+    dims,
+    latent_ref, context_ref, cond_ref, ccond_ref, modw_ref,
+    wq1_hbm, wq2_hbm, wk1_hbm, wk2_hbm, wv_hbm,
+    lam_ref, boost_ref, gain_ref, wo_hbm, crow_ref, srow_ref, ccol_ref, scol_ref,
+    out_ref,
+    wq1, wq2, wk1, wk2, wv, wo,
+    cos_ref, sin_ref, sig, modp, modall, modrow, lat, nrm, h,
+    qs, kvs, q, kv, mx, acc, ho, hr, rsend, rs,
+    wsem, mp_s, mp_r, lt_s, lt_r, ma_s, ma_r,
+    q_s, q_r, kz_s, kv_s, kv_r, ho_s, ho_r, rs_s, rs_r,
+):
+    S, T, G, R, B, Cr, cw = dims
+    s, t = lax.axis_index("sp"), lax.axis_index("tp")
+    g, r = s // R, s % R
+    rows, D = latent_ref.shape
+    Lr = rows * T
+    Cp = context_ref.shape[0]
+
+    def remote(src, dst, send, recv, sp, tp):
+        return pltpu.make_async_remote_copy(
+            src_ref=src, dst_ref=dst, send_sem=send, recv_sem=recv,
+            device_id=(sp, tp), device_id_type=MESH,
+        )
+
+    loads = [
+        pltpu.make_async_copy(a, b, wsem.at[i])
+        for i, (a, b) in enumerate(
+            [(wq1_hbm, wq1), (wq2_hbm, wq2), (wk1_hbm, wk1), (wk2_hbm, wk2), (wv_hbm, wv), (wo_hbm, wo)]
+        )
+    ]
+    for load in loads:
+        load.start()
+
+    barrier = pltpu.get_barrier_semaphore()
+
+    @pl.loop(1, S)
+    def _(i):
+        pl.semaphore_signal(barrier, inc=1, device_id=((s + i) % S, t), device_id_type=MESH)
+
+    for i in range(1, T):
+        pl.semaphore_signal(barrier, inc=1, device_id=(s, (t + i) % T), device_id_type=MESH)
+
+    for i in range(Lr // GRID_W):
+        span, at = slice(i * GRID_W, (i + 1) * GRID_W), pl.ds(s * (Lr // GRID_W) + i, 1)
+        cos_ref[span, :] = ccol_ref[...] + crow_ref[at, :]
+        sin_ref[span, :] = scol_ref[...] + srow_ref[at, :]
+    cos_ref[Lr:, :] = jnp.ones((Cp, LANES), F32)
+    sin_ref[Lr:, :] = jnp.zeros((Cp, LANES), F32)
+
+    for i, ref in enumerate((cond_ref, ccond_ref)):
+        v = ref[...]
+        sig[i : i + 1, :] = v / (1.0 + jnp.exp(-v))
+    modp[t] = jnp.dot(sig[...].astype(BF16), modw_ref[...], preferred_element_type=F32)
+
+    pl.semaphore_wait(barrier, S - 1 + T - 1)
+
+    def part_copy(i):
+        return remote(modp.at[t], modp.at[t], mp_s.at[i], mp_r.at[t], s, (t + i) % T)
+
+    def latent_copy(i):
+        return remote(latent_ref, lat.at[t], lt_s.at[i], lt_r.at[t], s, (t + i) % T)
+
+    for i in range(1, T):
+        part_copy(i).start()
+    for i in range(1, T):
+        latent_copy(i).start()
+    lat[t] = latent_ref[...]
+    for i in range(1, T):
+        o = (t + i) % T
+        remote(modp.at[o], modp.at[o], mp_s.at[i], mp_r.at[o], s, o).wait_recv()
+    total = modp[0]
+    for i in range(1, T):
+        total = total + modp[i]
+    modall[s] = total
+
+    def mod_copy(i, src):
+        return remote(modall.at[src], modall.at[src], ma_s.at[i], ma_r.at[src], (s + i) % S, t)
+
+    @pl.loop(1, S)
+    def _(i):
+        mod_copy(i, s).start()
+
+    for i in range(1, T):
+        o = (t + i) % T
+        remote(lat.at[o], lat.at[o], lt_s.at[i], lt_r.at[o], s, o).wait_recv()
+    step = math.gcd(rows, 32)
+    for i in range(T):
+
+        @pl.loop(0, rows // step)
+        def _(j):
+            at = pl.multiple_of(j * step, step)
+            nrm[pl.ds(i * rows + at, step), :] = normed_rows(lat[i, pl.ds(at, step), :])
+
+    nrm[Lr:, :] = normed_rows(context_ref[...])
+
+    @pl.loop(1, S)
+    def _(i):
+        mod_copy(i, (s + i) % S).wait_recv()
+
+    for i in range(S):
+        modrow[:, i * cw : (i + 1) * cw] = modall[i][:, :cw]
+
+    @pl.loop(0, Lr // step)
+    def _(j):
+        at = pl.ds(pl.multiple_of(j * step, step), step)
+        h[at, :] = (nrm[at, :] * (1.0 + modrow[0:1, D : 2 * D]) + modrow[0:1, :D]).astype(BF16)
+
+    h[Lr:, :] = (nrm[Lr:, :] * (1.0 + modrow[1:2, D : 2 * D]) + modrow[1:2, :D]).astype(BF16)
+
+    for i in range(2):
+        loads[i].wait()
+    lh = h[:Lr, :]
+    one = jnp.dot(lh, wq1[...], preferred_element_type=F32)
+    two = jnp.dot(lh, wq2[...], preferred_element_type=F32)
+    for i in range(G):
+        cut = slice(i * HEAD_DIM, (i + 1) * HEAD_DIM)
+        pair = jnp.concatenate([one[:, cut], two[:, cut]], axis=1)
+        turned = rotate(pair, cos_ref[:Lr, :], sin_ref[:Lr, :])
+        qs[i] = (turned * (LOG2E * HEAD_DIM**-0.5)).astype(BF16)
+
+    def q_out(i):
+        to = (g + i) % G
+        return remote(qs.at[to], q.at[g], q_s.at[i], q_r.at[g], to * R + r, t)
+
+    for i in range(1, G):
+        q_out(i).start()
+    q[g] = qs[g]
+
+    for i in range(2, 5):
+        loads[i].wait()
+    hh = h[...]
+    one = jnp.dot(hh, wk1[...], preferred_element_type=F32)
+    two = jnp.dot(hh, wk2[...], preferred_element_type=F32)
+    for i in range(G):
+        cut = slice(i * HEAD_DIM, (i + 1) * HEAD_DIM)
+        pair = jnp.concatenate([one[:, cut], two[:, cut]], axis=1)
+        kvs[i, :, :LANES] = rotate(pair, cos_ref[...], sin_ref[...]).astype(BF16)
+    val = jnp.dot(hh, wv[...], preferred_element_type=F32)
+    for i in range(G):
+        kvs[i, :, LANES:] = val[:, i * VALUE_DIM : (i + 1) * VALUE_DIM].astype(BF16)
+
+    def kv_out(i):
+        to = (g + i) % G
+        return remote(kvs.at[to], kv.at[s], kz_s.at[i], kv_r.at[s], to * R + r, t)
+
+    for i in range(1, G):
+        kv_out(i).start()
+    kv[s] = kvs[g]
+
+    def forward(i, j):
+        src = ((g + G - i) % G) * R + r
+        return remote(kv.at[src], kv.at[src], kv_s.at[i, j], kv_r.at[src], g * R + (r + j) % R, t)
+
+    def landed(src):
+        remote(kv.at[src], kv.at[src], kz_s.at[0], kv_r.at[src], s, t).wait_recv()
+
+    def forward_all(i):
+        @pl.loop(1, R)
+        def _(j):
+            forward(i, j).start()
+
+    forward_all(0)
+    mx[...] = jnp.full(mx.shape, NEGATIVE, F32)
+    acc[...] = jnp.zeros(acc.shape, F32)
+    boost = boost_ref[g] * LOG2E
+
+    for i in range(1, G):
+        o = (g + i) % G
+        remote(q.at[o], q.at[o], q_s.at[i], q_r.at[o], s, t).wait_recv()
+
+    def attend(n, at):
+        k_l = kv[pl.ds(at, B), :Lr, :LANES].reshape(B * Lr, LANES)
+        v_l = kv[pl.ds(at, B), :Lr, LANES:].reshape(B * Lr, VALUE_DIM)
+        k_c = kv[pl.ds(at, B), Lr:, :LANES].reshape(B * Cp, LANES)
+        v_c = kv[pl.ds(at, B), Lr:, LANES:].reshape(B * Cp, VALUE_DIM)
+        v_l = jnp.concatenate([v_l, jnp.ones_like(v_l)], axis=1)
+        v_c = jnp.concatenate([v_c, jnp.ones_like(v_c)], axis=1)
+        nt = (((1,), (1,)), ((), ()))
+        QB = min(Lr, QROWS)
+        for m, c in [(m, c) for c in range(Lr // QB) for m in range(2)]:
+            part = slice(c * QB, (c + 1) * QB)
+            qq = q[n, part, :]
+            lane = lax.broadcasted_iota(jnp.int32, qq.shape, 1)
+            qm = jnp.where(lane // HEAD_DIM == m, qq, jnp.zeros_like(qq))
+            s_l = lax.dot_general(qm, k_l, nt, preferred_element_type=F32)
+            s_c = lax.dot_general(qm, k_c, nt, preferred_element_type=F32) + boost
+            if Cp != Cr:
+                spot = lax.broadcasted_iota(jnp.int32, s_c.shape, 1)
+                s_c = jnp.where(spot % Cp < Cr, s_c, NEGATIVE)
+            old = mx[m, n, part, :]
+            peak = jnp.maximum(
+                old,
+                jnp.maximum(
+                    jnp.max(s_l, axis=-1, keepdims=True), jnp.max(s_c, axis=-1, keepdims=True)
+                ),
+            )
+            p_l = jnp.exp2(s_l - peak).astype(BF16)
+            p_c = jnp.exp2(s_c - peak).astype(BF16)
+            mx[m, n, part, :] = peak
+            acc[m, n, part, :] = (
+                jnp.exp2(old - peak) * acc[m, n, part, :]
+                + jnp.dot(p_l, v_l, preferred_element_type=F32)
+                + jnp.dot(p_c, v_c, preferred_element_type=F32)
+            )
+
+    lam = lam_ref[g]
+    gain = gain_ref[...]
+
+    def finish(n):
+        one = acc[0, n, :, :VALUE_DIM] / acc[0, n, :, VALUE_DIM:]
+        two = acc[1, n, :, :VALUE_DIM] / acc[1, n, :, VALUE_DIM:]
+        mixed = one - lam * two
+        mixed = mixed * lax.rsqrt(jnp.mean(mixed * mixed, axis=-1, keepdims=True) + EPSILON) * gain
+        return mixed.astype(BF16)
+
+    def ho_out(i):
+        to = (g + i) % G
+        return remote(ho.at[to], hr.at[g], ho_s.at[i], ho_r.at[g], to * R + r, t)
+
+    def pass_on(i):
+        landed(((g + G - i) % G) * R + r)
+        forward_all(i)
+
+    for i in range(G):
+        if i == 1 and G > 2:
+            pass_on(2)
+        base = ((g + G - i) % G) * R
+
+        @pl.loop(1, R)
+        def _(j):
+            landed(base + (r + j) % R)
+
+        if i + 1 < G:
+            half = G // 2
+            for low, high in ((0, half), (half, G)):
+                if low and i == 0:
+                    pass_on(1)
+                elif low and i + 2 < G:
+                    pass_on(i + 2)
+
+                @pl.loop(low * (R // B), high * (R // B))
+                def _(x):
+                    attend(x // (R // B), base + x % (R // B) * B)
+
+        else:
+
+            @pl.loop(1, G + 1)
+            def _(y):
+                n = (g + y) % G
+
+                @pl.loop(0, R // B)
+                def _(x):
+                    attend(n, base + x * B)
+
+                ho[n] = finish(n)
+
+                @pl.when(y < G)
+                def _():
+                    ho_out(y).start()
+
+    hr[g] = ho[g]
+    loads[5].wait()
+    for i in range(1, G):
+        o = (g + i) % G
+        remote(hr.at[o], hr.at[o], ho_s.at[i], ho_r.at[o], s, t).wait_recv()
+
+    def branch_rows(o):
+        at = pl.multiple_of(o * rows, rows)
+        mine = jnp.concatenate([hr[i, pl.ds(at, rows), :] for i in range(G)], axis=1)
+        return jnp.dot(mine, wo[...], preferred_element_type=F32)
+
+    def rs_out(i):
+        o = (t + i) % T
+        return remote(rsend.at[o], rs.at[t], rs_s.at[i], rs_r.at[t], s, o)
+
+    for i in range(1, T):
+        o = (t + i) % T
+        rsend[o] = branch_rows(o).astype(BF16)
+        rs_out(i).start()
+    branch = branch_rows(t)
+    for i in range(1, T):
+        o = (t + i) % T
+        remote(rs.at[o], rs.at[o], rs_s.at[i], rs_r.at[o], s, o).wait_recv()
+        branch = branch + rs[o].astype(F32)
+    out_ref[...] = (latent_ref[...].astype(F32) + modrow[0:1, 2 * D :] * branch).astype(BF16)
+
+    for i in range(1, T):
+        part_copy(i).wait_send()
+        latent_copy(i).wait_send()
+        rs_out(i).wait_send()
+
+    @pl.loop(1, S)
+    def _(i):
+        mod_copy(i, s).wait_send()
+
+    for i in range(1, G):
+        kv_out(i).wait_send()
+        q_out(i).wait_send()
+        ho_out(i).wait_send()
+    for i in range(G):
+
+        @pl.loop(1, R)
+        def _(j):
+            forward(i, j).wait_send()
+
+
+def general_body(
+    S, T,
+    latent, context, condition, context_condition, modulation_weight,
+    query_first, query_second, key_first, key_second, value_weight,
+    lambda_head, context_score_boost, head_gain, output_weight,
+):
+    rows, D = latent.shape
+    Lr = rows * T
+    G = value_weight.shape[1] // VALUE_DIM
+    assert S % G == 0
+    R = S // G
+    B = math.gcd(R, 4)
+    Cr = context.shape[0]
+    Cp = -(-Cr // 16) * 16
+    if Cp != Cr:
+        context = jnp.pad(context, ((0, Cp - Cr), (0, 0)))
+    cw = modulation_weight.shape[1]
+    cp = -(-cw // LANES) * LANES
+    if cp != cw:
+        modulation_weight = jnp.pad(modulation_weight, ((0, 0), (0, cp - cw)))
+    depth = modulation_weight.shape[0]
+    assert Lr % GRID_W == 0
+    tables = rotation_tables(S * Lr // GRID_W)
+    vm = pl.BlockSpec(memory_space=pltpu.VMEM)
+    sm = pl.BlockSpec(memory_space=pltpu.SMEM)
+    hb = pl.BlockSpec(memory_space=pl.ANY)
+    V = pltpu.VMEM
+    dma = pltpu.SemaphoreType.DMA
+    weights = (query_first, query_second, key_first, key_second, value_weight, output_weight)
+    return pl.pallas_call(
+        functools.partial(general_kernel, (S, T, G, R, B, Cr, cw)),
+        out_shape=jax.ShapeDtypeStruct((rows, D), BF16),
+        in_specs=[vm] * 5 + [hb] * 5 + [sm, sm, vm, hb, vm, vm, vm, vm],
+        out_specs=vm,
+        scratch_shapes=[V(w.shape, BF16) for w in weights]
+        + [
+            V((Lr + Cp, LANES), F32),
+            V((Lr + Cp, LANES), F32),
+            V((2, depth), F32),
+            V((T, 2, cp), F32),
+            V((S, 2, cp), F32),
+            V((2, 3 * D), F32),
+            V((T, rows, D), BF16),
+            V((Lr + Cp, D), F32),
+            V((Lr + Cp, D), BF16),
+            V((G, Lr, LANES), BF16),
+            V((G, Lr + Cp, LANES + VALUE_DIM), BF16),
+            V((G, Lr, LANES), BF16),
+            V((S, Lr + Cp, LANES + VALUE_DIM), BF16),
+            V((2, G, Lr, 1), F32),
+            V((2, G, Lr, 2 * VALUE_DIM), F32),
+            V((G, Lr, VALUE_DIM), BF16),
+            V((G, Lr, VALUE_DIM), BF16),
+            V((T, rows, D), BF16),
+            V((T, rows, D), BF16),
+            dma((6,)),
+            dma((T,)), dma((T,)), dma((T,)), dma((T,)), dma((S,)), dma((S,)),
+            dma((G,)), dma((G,)), dma((G,)), dma((G, R)), dma((S,)),
+            dma((G,)), dma((G,)), dma((T,)), dma((T,)),
         ],
         compiler_params=pltpu.CompilerParams(
             collective_id=0, has_side_effects=True, vmem_limit_bytes=62 * 1024 * 1024
@@ -669,5 +1027,6 @@
         P("tp", None),
     )
     out_specs = P(("sp", "tp"), None)
-    run = functools.partial(body, mesh.shape["sp"], mesh.shape["tp"])
+    S, T = mesh.shape["sp"], mesh.shape["tp"]
+    run = functools.partial(body if T == 2 else general_body, S, T)
     return jax.shard_map(run, mesh=mesh, in_specs=in_specs, out_specs=out_specs, check_vma=False)

time: 65.9 us -> 58 us (0.88)
  Pallas kernels: 63.1 us -> 55.2 us
    pallas_call x1, Pallas kernels: 63.1 us -> 55.2 us  [body(): pl.pallas_call(functools.partial(kernel, (S, T, G, R, Cr, cw)), out_shape...]
where the time goes in v3:
time: 58 us; the launch traced here: 57.1 us
  Pallas kernels  55.2 us (95%)
  local copies, waits for them, and re-layouts  1.88 us (3%)
    pallas_call x1, Pallas kernels, body(): pl.pallas_call(functools.partial(kernel, (S, T, G, R, Cr, cw)), out_shape...  55.2 us
    unnamed x1, local copies, waits for them, and re-layouts  1.88 us

profile of v3, /device:TPU:1, one launch (start us, length us, event | category | flops | bytes accessed | tf_op | source)
XLA Modules:
  0.0 57.1 jit_solution(18324177346570300229)
XLA Ops:
  0.0 55.2 %shard_map.172 = bf16[128,2048]{1,0:T(8,128)(2,1)} custom-call(bf16[128,2048]{1,0:T(8,128)(2,1)} %lat_hbm.1, bf16[32,2048]{1,0:T(8,128)(2,1)} %ctx_hbm.1, f32[1,1024]{1,0:T(1,128)} %bitcast.3, f32[1,1024]{1,0:T(1,128)} %bitcast.4, bf16[1024,384]{1,0:T(8,128)(2,1)} %modw_hbm.1, bf16[2048,256]{1,0:T(8,128)(2,1)} %wq1_hbm.1, bf16[2048,256]{1,0:T(8,128)(2,1)} %wq2_hbm.1, ...), custom_call_target="tpu_custom_call" | custom-call | tf_op jit(solution)/shard_map/pallas_call | solution.py:576
  55.2 1.9 %copy.20 = bf16[128,2048]{1,0:T(8,128)(2,1)} copy(bf16[128,2048]{1,0:T(8,128)(2,1)} %shard_map.172) | data formatting | bytes 1048576

commit v4 on v3

--- a/solution.py
+++ b/solution.py
@@ -71,9 +71,9 @@
     lam_ref, boost_ref, gain_ref, wo_hbm, crow_ref, srow_ref, ccol_ref, scol_ref,
     out_ref,
     wq1, wq2, wk1, wk2, wv, wo,
-    ctx, cond, modw, tab, cos_ref, sin_ref, mp, modrow, lat, raw, nrm, h, hraw,
-    qs, kvs, kvrs, q, qb, kvn, kvr, kvf, s0, s1, vt0, vt1, pk0, pk1, mx, acc, ho, hr, lb,
-    wsem, isem, mp_s, mp_r, lt_s, lt_r, lb_s, lb_r, wo_s, wo_r,
+    ctx, cond, modw, tab, cos_ref, sin_ref, mt, mp, modrow, lat, raw, nrm, h, hraw,
+    qs, kvs, kvrs, q, qb, kvn, kvr, kvf, s0, s1, vt0, pk0, mx, acc, ho, hr, lb,
+    wsem, isem, mt_s, mt_r, mp_s, mp_r, lt_s, lt_r, lb_s, lb_r, wo_s, wo_r,
     rw_s, rw_r, rf_s, rf_r, q_s, q_r, kn_s, kn_r, kf_s, kf_r, kr_s, kr_r, fn_s, ff_s, fr_s, ho_s, ho_r,
 ):
     S, T, G, R, Cr, cw = dims
@@ -103,14 +103,14 @@
     def arrived(buf, recv):
         remote(buf, buf, lt_s.at[0], recv, s, t).wait_recv()
 
-    f0 = s * T + t
-    F = S * T
     barrier = pltpu.get_barrier_semaphore()
 
-    @pl.loop(1, F)
+    @pl.loop(1, S)
     def _(i):
-        f = (f0 + i) % F
-        pl.semaphore_signal(barrier, inc=1, device_id=(f // T, f % T), device_id_type=MESH)
+        pl.semaphore_signal(barrier, inc=1, device_id=((s + i) % S, t), device_id_type=MESH)
+
+    for i in range(1, T):
+        pl.semaphore_signal(barrier, inc=1, device_id=(s, (t + i) % T), device_id_type=MESH)
 
     inputs = [
         pltpu.make_async_copy(a, b, isem.at[i])
@@ -138,15 +138,17 @@
         inputs[i].wait()
     v = cond[...]
     sig = v / (1.0 + jnp.exp(-v))
-    mp[f0] = jnp.dot(sig.astype(BF16), modw[...], preferred_element_type=F32)
+    mt[t] = jnp.dot(sig.astype(BF16), modw[...], preferred_element_type=F32)
     for i in range(3, 5):
         inputs[i].wait()
 
-    pl.semaphore_wait(barrier, F - 1)
+    pl.semaphore_wait(barrier, S - 1 + T - 1)
+
+    def mt_copy(i):
+        return remote(mt.at[t], mt.at[t], mt_s.at[i], mt_r.at[t], s, (t + i) % T)
 
     def mp_copy(i):
-        f = (f0 + i) % F
-        return remote(mp.at[f0], mp.at[f0], mp_s.at[i], mp_r.at[f0], f // T, f % T)
+        return remote(mp.at[s], mp.at[s], mp_s.at[i], mp_r.at[s], (s + i) % S, t)
 
     def lat_copy(i):
         return remote(lat.at[t], lat.at[t], lt_s.at[i], lt_r.at[t], s, (t + i) % T)
@@ -169,7 +171,17 @@
             part, part, rf_s.at[j - 1, c, i], rf_r.at[j - 1, c, t], s, (t + i) % T
         )
 
-    @pl.loop(1, F)
+    for i in range(1, T):
+        mt_copy(i).start()
+    for i in range(1, T):
+        o = (t + i) % T
+        arrived(mt.at[o], mt_r.at[o])
+    total = mt[0]
+    for i in range(1, T):
+        total = total + mt[i]
+    mp[s] = total
+
+    @pl.loop(1, S)
     def _(i):
         mp_copy(i).start()
 
@@ -220,16 +232,13 @@
         arrived(lat.at[o], lt_r.at[o])
         norm_lat(o)
 
-    @pl.loop(1, F)
+    @pl.loop(1, S)
     def _(i):
-        f = (f0 + i) % F
-        arrived(mp.at[f], mp_r.at[f])
+        o = (s + i) % S
+        arrived(mp.at[o], mp_r.at[o])
 
     for i in range(S):
-        total = mp[i * T]
-        for j in range(1, T):
-            total = total + mp[i * T + j]
-        modrow[:, i * cw : (i + 1) * cw] = total[:, :cw]
+        modrow[:, i * cw : (i + 1) * cw] = mp[i][:, :cw]
 
     @pl.loop(0, Lr // step)
     def _(j):
@@ -357,8 +366,7 @@
 
     mx[...] = jnp.full(mx.shape, NEGATIVE, F32)
     acc[...] = jnp.zeros(acc.shape, F32)
-    for vt in (vt0, vt1):
-        vt[VALUE_DIM:, :] = jnp.ones((vt.shape[0] - VALUE_DIM, vt.shape[1]), BF16)
+    vt0[VALUE_DIM:, :] = jnp.ones((vt0.shape[0] - VALUE_DIM, vt0.shape[1]), BF16)
     for i in range(1, T):
         o = (t + i) % T
         arrived(lb.at[o], lb_r.at[o])
@@ -393,36 +401,43 @@
             for slot in slots:
                 arrived(buf.at[slot], recv.at[slot])
 
-    def scores(buf, base, count, low, s_ref, vt_ref, pk_ref):
-        span = buf.shape[1]
+    half = N // 2
+    banks = (s0, s1)
+
+    def scores(buf, base, count, low, c):
+        cols = slice(c * half, (c + 1) * half)
         at = pl.ds(base, count)
-        keys = buf[at, :low, :LANES].reshape(count * low, LANES)
-        vals = buf[at, :low, LANES:].reshape(count * low, VALUE_DIM)
-        sc = lax.dot_general(keys, qb[...], nt, preferred_element_type=F32)
         n = count * low
+        m = count * (buf.shape[1] - low)
+        s_ref, vt = banks[c], vt0
+        keys = buf[at, :low, :LANES].reshape(n, LANES)
+        sc = lax.dot_general(keys, qb[cols, :], nt, preferred_element_type=F32)
         s_ref[:n, :] = sc
         peak = jnp.max(sc, axis=0, keepdims=True)
-        vt_ref[:VALUE_DIM, :n] = vals.astype(F32).T.astype(BF16)
-        if span > low:
-            m = count * (span - low)
+        if c == 0:
+            vals = buf[at, :low, LANES:].reshape(n, VALUE_DIM)
+            vt[:VALUE_DIM, :n] = vals.astype(F32).T.astype(BF16)
+        if m:
             keys = buf[at, low:, :LANES].reshape(m, LANES)
-            vals = buf[at, low:, LANES:].reshape(m, VALUE_DIM)
-            sc = lax.dot_general(keys, qb[...], nt, preferred_element_type=F32) + boost
+            sc = lax.dot_general(keys, qb[cols, :], nt, preferred_element_type=F32) + boost
             if Cp != Cr:
                 spot = lax.broadcasted_iota(jnp.int32, sc.shape, 0)
                 sc = jnp.where(spot % Cp < Cr, sc, NEGATIVE)
             s_ref[n : n + m, :] = sc
             peak = jnp.maximum(peak, jnp.max(sc, axis=0, keepdims=True))
-            vt_ref[:VALUE_DIM, n : n + m] = vals.astype(F32).T.astype(BF16)
-        pk_ref[...] = peak
-
-    def weigh(n, s_ref, vt_ref, pk_ref):
-        old = mx[...]
-        peak = jnp.maximum(old, pk_ref[...])
-        pr = jnp.exp2(s_ref[:n, :] - peak).astype(BF16)
-        mx[...] = peak
-        acc[...] = jnp.exp2(old - peak) * acc[...] + jnp.dot(
-            vt_ref[:, :n], pr, preferred_element_type=F32
+            if c == 0:
+                vals = buf[at, low:, LANES:].reshape(m, VALUE_DIM)
+                vt[:VALUE_DIM, n : n + m] = vals.astype(F32).T.astype(BF16)
+        pk0[:, cols] = peak
+
+    def weigh(n, c):
+        cols = slice(c * half, (c + 1) * half)
+        old = mx[:, cols]
+        peak = jnp.maximum(old, pk0[:, cols])
+        pr = jnp.exp2(banks[c][:n, :] - peak).astype(BF16)
+        mx[:, cols] = peak
+        acc[:, cols] = jnp.exp2(old - peak) * acc[:, cols] + jnp.dot(
+            vt0[:, :n], pr, preferred_element_type=F32
         )
 
     def finish(j):
@@ -456,27 +471,29 @@
             units.append((kvf, base, wide, Lr - Rr, ff_s, kf_r, False))
     for k in range(P // quad):
         units.append((kvr, flip(p0 // quad, k, P // quad) * quad, quad, Q * Rr, fr_s, kr_r, True))
-    banks = ((s0, vt0, pk0), (s1, vt1, pk1))
-    last = None
+    def deliver(c):
+        for j in range(c * P // 2, (c + 1) * P // 2):
+            finish(j)
+
+            @pl.when(p0 == j)
+            def _():
+                hr[j] = ho[j]
+
+            @pl.when(p0 != j)
+            def _():
+                ho_out(j).start()
+
     for n, (buf, base, count, low, send, recv, own) in enumerate(units):
         spread(buf, [base + i for i in range(count)], send, recv, own)
         settle(buf, [base + i for i in range(count)], recv)
-        scores(buf, base, count, low, *banks[n % 2])
-        if last is not None:
-            weigh(last, *banks[(n - 1) % 2])
-        last = count * buf.shape[1]
-    weigh(last, *banks[(len(units) - 1) % 2])
-
-    for j in range(P):
-        finish(j)
-
-        @pl.when(p0 == j)
-        def _():
-            hr[j] = ho[j]
-
-        @pl.when(p0 != j)
-        def _():
-            ho_out(j).start()
+        size = count * buf.shape[1]
+        scores(buf, base, count, low, 0)
+        scores(buf, base, count, low, 1)
+        weigh(size, 0)
+        if n == len(units) - 1:
+            deliver(0)
+        weigh(size, 1)
+    deliver(1)
 
     for i in range(1, T):
         o = (t + i) % T
@@ -492,7 +509,10 @@
         branch = term if branch is None else branch + term
     out_ref[...] = (lat[t].astype(F32) + modrow[0:1, 2 * D :] * branch).astype(BF16)
 
-    @pl.loop(1, F)
+    for i in range(1, T):
+        mt_copy(i).wait_send()
+
+    @pl.loop(1, S)
     def _(i):
         mp_copy(i).wait_send()
 
@@ -563,7 +583,7 @@
     tables = rotation_tables(S * Lr // GRID_W)
     vm = pl.BlockSpec(memory_space=pltpu.VMEM)
     sm = pl.BlockSpec(memory_space=pltpu.SMEM)
-    hb = pl.BlockSpec(memory_space=pl.ANY)
+    hb = pl.BlockSpec(memory_space=pltpu.HBM)
     V = pltpu.VMEM
     dma = pltpu.SemaphoreType.DMA
     keys = Lr + Cp
@@ -573,9 +593,14 @@
     quad, wide = groups(P, Q * Rr, keys - Rr)
     most = max(2 * keys, quad * Q * Rr, wide * (keys - Rr))
     weights = (query_first, query_second, key_first, key_second, value_weight)
+    latent, context, modulation_weight, output_weight, *weights = (
+        pltpu.with_memory_space_constraint(a, pltpu.HBM)
+        for a in (latent, context, modulation_weight, output_weight, *weights)
+    )
+    query_first, query_second, key_first, key_second, value_weight = weights
     return pl.pallas_call(
         functools.partial(kernel, (S, T, G, R, Cr, cw)),
-        out_shape=jax.ShapeDtypeStruct((rows, D), BF16),
+        out_shape=pltpu.VMEM((rows, D), BF16),
         in_specs=[hb] * 10 + [sm, sm, vm, hb, vm, vm, vm, vm],
         out_specs=vm,
         scratch_shapes=[V(w.shape, BF16) for w in weights]
@@ -587,7 +612,8 @@
             V((2, Lr, LANES), F32),
             V((keys + Q * Rr, LANES), F32),
             V((keys + Q * Rr, LANES), F32),
-            V((S * T, 2, cp), F32),
+            V((T, 2, cp), F32),
+            V((S, 2, cp), F32),
             V((2, 3 * D), F32),
             V((T, rows, D), BF16),
             V((Q, T, chunks, rc, D), BF16),
@@ -602,11 +628,9 @@
             V((P, keys, pairw), BF16),
             V((P, Q * Rr, pairw), BF16),
             V((Q * P, keys - Rr, pairw), BF16),
-            V((most, N), F32),
-            V((most, N), F32),
+            V((most, N // 2), F32),
+            V((most, N // 2), F32),
             V((VALUE_DIM + 16, most), BF16),
-            V((VALUE_DIM + 16, most), BF16),
-            V((1, N), F32),
             V((1, N), F32),
             V((1, N), F32),
             V((VALUE_DIM + 16, N), F32),
@@ -614,7 +638,7 @@
             V((P, rows, VALUE_DIM), BF16),
             V((T, 2 * G, LANES), F32),
             dma((6,)), dma((5,)),
-            dma((S * T,)), dma((S * T,)),
+            dma((T,)), dma((T,)), dma((S,)), dma((S,)),
             dma((T,)), dma((T,)), dma((T,)), dma((T,)), dma((T,)), dma((T,)),
             dma((Q, chunks)), dma((Q, chunks)), dma((Q, chunks, T)), dma((Q, chunks, T)),
             dma((G, T)), dma((P,)),
@@ -623,7 +647,7 @@
             dma((P,)), dma((P,)),
         ],
         compiler_params=pltpu.CompilerParams(
-            collective_id=0, has_side_effects=True, vmem_limit_bytes=62 * 1024 * 1024
+            collective_id=0, has_side_effects=True, vmem_limit_bytes=56 * 1024 * 1024
         ),
     )(
         latent, context, condition[None, :], context_condition[None, :], modulation_weight,

time: 58 us -> 53.7 us (0.926)
  the two profiles are of different devices: /device:TPU:1 before, /device:TPU:20 now
where the time goes in v4:
time: 53.7 us; the launch traced here: 53.5 us
  Pallas kernels  52.7 us (98%)
  local copies, waits for them, and re-layouts  0.8 us (1%)
    pallas_call x1, Pallas kernels, body(): pl.pallas_call(functools.partial(kernel, (S, T, G, R, Cr, cw)), out_shape...  52.7 us

profile of v4, /device:TPU:20, one launch (start us, length us, event | category | flops | bytes accessed | tf_op | source)
XLA Modules:
  0.0 53.5 jit_solution(12868550153607395660)
XLA Ops:
  0.0 52.7 %shard_map.172 = bf16[128,2048]{1,0:T(8,128)(2,1)S(1)} custom-call(bf16[128,2048]{1,0:T(8,128)(2,1)} %lat_hbm.1, bf16[32,2048]{1,0:T(8,128)(2,1)} %ctx_hbm.1, f32[1,1024]{1,0:T(1,128)} %bitcast.3, f32[1,1024]{1,0:T(1,128)} %bitcast.4, bf16[1024,384]{1,0:T(8,128)(2,1)} %modw_hbm.1, bf16[2048,256]{1,0:T(8,128)(2,1)} %wq1_hbm.1, bf16[2048,256]{1,0:T(8,128)(2,1)} %wq2_hbm.1, ...), custom_call_target="tpu_custom_call" | custom-call | tf_op jit(solution)/shard_map/pallas_call | solution.py:601
  52.7 0.8 %copy.20 = bf16[128,2048]{1,0:T(8,128)(2,1)} copy(bf16[128,2048]{1,0:T(8,128)(2,1)S(1)} %shard_map.172) | data formatting | bytes 1048576

commit v5 on v4

--- a/solution.py
+++ b/solution.py
@@ -173,6 +173,8 @@
 
     for i in range(1, T):
         mt_copy(i).start()
+    for j in range(1, R):
+        raw_copy(j, 0).start()
     for i in range(1, T):
         o = (t + i) % T
         arrived(mt.at[o], mt_r.at[o])
@@ -188,7 +190,7 @@
     for i in range(1, T):
         lat_copy(i).start()
         lb_copy(i).start()
-    for c in range(chunks):
+    for c in range(1, chunks):
         for j in range(1, R):
             raw_copy(j, c).start()
     loads[5].wait()
@@ -411,23 +413,22 @@
         m = count * (buf.shape[1] - low)
         s_ref, vt = banks[c], vt0
         keys = buf[at, :low, :LANES].reshape(n, LANES)
+        vals = buf[at, :low, LANES:].reshape(n, VALUE_DIM)
+        if m:
+            keys = jnp.concatenate([keys, buf[at, low:, :LANES].reshape(m, LANES)], axis=0)
+            vals = jnp.concatenate([vals, buf[at, low:, LANES:].reshape(m, VALUE_DIM)], axis=0)
+        if c == 0:
+            vt[:VALUE_DIM, : n + m] = vals.astype(F32).T.astype(BF16)
         sc = lax.dot_general(keys, qb[cols, :], nt, preferred_element_type=F32)
-        s_ref[:n, :] = sc
-        peak = jnp.max(sc, axis=0, keepdims=True)
-        if c == 0:
-            vals = buf[at, :low, LANES:].reshape(n, VALUE_DIM)
-            vt[:VALUE_DIM, :n] = vals.astype(F32).T.astype(BF16)
+        s_ref[:n, :] = sc[:n]
+        peak = jnp.max(sc[:n], axis=0, keepdims=True)
         if m:
-            keys = buf[at, low:, :LANES].reshape(m, LANES)
-            sc = lax.dot_general(keys, qb[cols, :], nt, preferred_element_type=F32) + boost
+            lifted = sc[n:] + boost
             if Cp != Cr:
-                spot = lax.broadcasted_iota(jnp.int32, sc.shape, 0)
-                sc = jnp.where(spot % Cp < Cr, sc, NEGATIVE)
-            s_ref[n : n + m, :] = sc
-            peak = jnp.maximum(peak, jnp.max(sc, axis=0, keepdims=True))
-            if c == 0:
-                vals = buf[at, low:, LANES:].reshape(m, VALUE_DIM)
-                vt[:VALUE_DIM, n : n + m] = vals.astype(F32).T.astype(BF16)
+                spot = lax.broadcasted_iota(jnp.int32, lifted.shape, 0)
+                lifted = jnp.where(spot % Cp < Cr, lifted, NEGATIVE)
+            s_ref[n : n + m, :] = lifted
+            peak = jnp.maximum(peak, jnp.max(lifted, axis=0, keepdims=True))
         pk0[:, cols] = peak
 
     def weigh(n, c):

time: 53.7 us -> 52.9 us (0.985)
  the two profiles are of different devices: /device:TPU:20 before, /device:TPU:1 now
where the time goes in v5:
time: 52.9 us; the launch traced here: 52.2 us
  Pallas kernels  51.4 us (97%)
  local copies, waits for them, and re-layouts  0.8 us (2%)
    pallas_call x1, Pallas kernels, body(): pl.pallas_call(functools.partial(kernel, (S, T, G, R, Cr, cw)), out_shape...  51.4 us

profile of v5, /device:TPU:1, one launch (start us, length us, event | category | flops | bytes accessed | tf_op | source)
XLA Modules:
  0.0 52.2 jit_solution(3171892386977970614)
XLA Ops:
  0.0 51.4 %shard_map.172 = bf16[128,2048]{1,0:T(8,128)(2,1)S(1)} custom-call(bf16[128,2048]{1,0:T(8,128)(2,1)} %lat_hbm.1, bf16[32,2048]{1,0:T(8,128)(2,1)} %ctx_hbm.1, f32[1,1024]{1,0:T(1,128)} %bitcast.3, f32[1,1024]{1,0:T(1,128)} %bitcast.4, bf16[1024,384]{1,0:T(8,128)(2,1)} %modw_hbm.1, bf16[2048,256]{1,0:T(8,128)(2,1)} %wq1_hbm.1, bf16[2048,256]{1,0:T(8,128)(2,1)} %wq2_hbm.1, ...), custom_call_target="tpu_custom_call" | custom-call | tf_op jit(solution)/shard_map/pallas_call | solution.py:602
  51.4 0.8 %copy.20 = bf16[128,2048]{1,0:T(8,128)(2,1)} copy(bf16[128,2048]{1,0:T(8,128)(2,1)S(1)} %shard_map.172) | data formatting | bytes 1048576

commit v6 on v5

--- a/solution.py
+++ b/solution.py
@@ -499,14 +499,17 @@
     for i in range(1, T):
         o = (t + i) % T
         arrived(wo.at[o], wo_r.at[o])
-    for i in range(1, P):
-        o = flip(p0, i, P)
-        arrived(hr.at[o], ho_r.at[o])
-
     branch = None
     for i in range(T):
-        part = jnp.concatenate([hr[i * G + j] for j in range(G)], axis=1)
-        term = jnp.dot(part, wo[i], preferred_element_type=F32)
+        side = (prim + i) % T
+        for j in range(G):
+            if i:
+                arrived(hr.at[side * G + j], ho_r.at[side * G + j])
+            elif j:
+                o = prim * G + flip(hown, j, G)
+                arrived(hr.at[o], ho_r.at[o])
+        part = jnp.concatenate([hr[side * G + j] for j in range(G)], axis=1)
+        term = jnp.dot(part, wo[side], preferred_element_type=F32)
         branch = term if branch is None else branch + term
     out_ref[...] = (lat[t].astype(F32) + modrow[0:1, 2 * D :] * branch).astype(BF16)
 

time: 52.9 us -> 52.9 us (level)
  no operation moved by 1% of the time
where the time goes in v6:
time: 52.9 us; the launch traced here: 52.4 us
  Pallas kernels  51.6 us (98%)
  local copies, waits for them, and re-layouts  0.8 us (2%)
    pallas_call x1, Pallas kernels, body(): pl.pallas_call(functools.partial(kernel, (S, T, G, R, Cr, cw)), out_shape...  51.6 us

profile of v6, /device:TPU:1, one launch (start us, length us, event | category | flops | bytes accessed | tf_op | source)
XLA Modules:
  0.0 52.4 jit_solution(17476802733071847470)
XLA Ops:
  0.0 51.6 %shard_map.172 = bf16[128,2048]{1,0:T(8,128)(2,1)S(1)} custom-call(bf16[128,2048]{1,0:T(8,128)(2,1)} %lat_hbm.1, bf16[32,2048]{1,0:T(8,128)(2,1)} %ctx_hbm.1, f32[1,1024]{1,0:T(1,128)} %bitcast.3, f32[1,1024]{1,0:T(1,128)} %bitcast.4, bf16[1024,384]{1,0:T(8,128)(2,1)} %modw_hbm.1, bf16[2048,256]{1,0:T(8,128)(2,1)} %wq1_hbm.1, bf16[2048,256]{1,0:T(8,128)(2,1)} %wq2_hbm.1, ...), custom_call_target="tpu_custom_call" | custom-call | tf_op jit(solution)/shard_map/pallas_call | solution.py:605
  51.6 0.8 %copy.20 = bf16[128,2048]{1,0:T(8,128)(2,1)} copy(bf16[128,2048]{1,0:T(8,128)(2,1)S(1)} %shard_map.172) | data formatting | bytes 1048576
